TPU v7x, 256 devices: a whole 4x4x8 slice. The times are simulated.
256 devices in a mesh: kv: 32 (over z, x), tp: 8 (over y, core).
Axes of the slice: x: 4, y: 4, z: 8, core: 2. Of those that a mesh axis runs over, the one named last changes fastest.
Arguments:
- tokens: bfloat16 [384, 2048], P(None, 'kv'), may hold values from -40 to 40
- norm_gain: float32 [2048], P('kv'), may hold values from 0.1 to 1.9
- w_query: bfloat16 [2048, 1024], P('kv', 'tp'), may hold values from -0.088388348 to 0.088388348
- w_key: bfloat16 [2048, 1024], P('kv', 'tp'), may hold values from -0.125 to 0.125
- w_value: bfloat16 [2048, 1024], P('kv', 'tp'), may hold values from -0.125 to 0.125
- w_gate: bfloat16 [2048, 16], replicated, may hold values from -0.125 to 0.125
- gate_bias: float32 [16], replicated, may hold values from -1 to 3
- w_out: bfloat16 [1024, 2048], P('tp', 'kv'), may hold values from -0.1875 to 0.1875
- keys_cache: bfloat16 [24, 16384, 1024], P(None, 'kv', 'tp'), may hold values from -512 to 512
- values_cache: bfloat16 [24, 16384, 1024], P(None, 'kv', 'tp'), may hold values from -6 to 6
- cum_gates: float32 [24, 16, 16384], P(None, 'tp', 'kv'), may hold values from -16784 to 0, as said below
- prior_len: int32 [24], replicated, may hold values from 8192 to 16362, as said below
- accepted: int32 [24], replicated, may hold values from 0 to 6
- parents: int32 [24, 16], replicated, may hold values from -1 to 14, as said below
Outputs:
- mixed_rows: bfloat16 [384, 2048], P('tp', 'kv')
- keys_out: bfloat16 [24, 16384, 1024], P(None, 'kv', 'tp')
- values_out: bfloat16 [24, 16384, 1024], P(None, 'kv', 'tp')
Inputs may be any that keep to these rules, and one draw needn't show every extreme that they name: parents[b, 0] = -1 and 0 <= parents[b, j] < j for later j. prior_len is at least half of 16384, and prior_len + accepted + 16 <= 16384. `cum_gates`: non-increasing along positions.
All inputs are finite; a program needn't handle non-finite values.
Results may differ from a plain program's by a relative error of at most 0.04.
Values may be sent and summed in bfloat16 or wider, within the bound.
A program may use at most 64 MiB of HBM per device.

v0:
```python
import jax
import jax.numpy as jnp
from jax import lax
from jax.sharding import Mesh
from jax.sharding import PartitionSpec as P

D = 2048
HEAD = 64
PROPS = 16
KV = ("kv_0", "kv_1")


masked_score = -1e30
norm_eps = 1e-06


def from_everyone(shard, axis):
    count = lax.axis_size(axis)
    return lax.all_to_all(
        jnp.broadcast_to(shard[None], (count, *shard.shape)), axis, 0, 0, tiled=True
    )


def of_everyone(shard, axis):
    return from_everyone(shard, axis).sum(axis=0)


def in_one(arrays, axis):
    ends = [0]
    for a in arrays:
        ends.append(ends[-1] + a.size)
    running = of_everyone(jnp.concatenate([a.ravel() for a in arrays]), axis)
    return tuple((running[b:e].reshape(a.shape) for a, b, e in zip(arrays, ends, ends[1:])))


def in_blocks(shard, dim, count):
    lengths = shard.shape
    blocks = shard.reshape(*lengths[:dim], count, lengths[dim] // count, *lengths[dim + 1 :])
    return jnp.moveaxis(blocks, dim, 0)


def summed_on_arrival(shard, axis, dim):
    count = lax.axis_size(axis)
    blocks = lax.all_to_all(in_blocks(shard, dim, count), axis, 0, 0, tiled=True)
    return jnp.sum(blocks.astype(jnp.float32), axis=0)


def joined_along(blocks, dim):
    blocks = jnp.moveaxis(blocks, 0, dim)
    lengths = blocks.shape
    return blocks.reshape(*lengths[:dim], lengths[dim] * lengths[dim + 1], *lengths[dim + 2 :])


def collect(shard, axis, dim):
    blocks = from_everyone(shard, axis)
    return joined_along(blocks, dim)


def collected_together(shard, axis):
    leaves = jax.tree.leaves(shard)
    sequence = sorted(range(len(leaves)), key=lambda k: -leaves[k].size)
    width = (1, *leaves[sequence[0]].shape)[-1]
    lines = [
        jnp.pad(leaves[k].reshape(-1), (0, -leaves[k].size % width)).reshape(-1, width)
        for k in sequence
    ]
    both, at, found = (lax.all_gather(jnp.concatenate(lines), axis), 0, {})
    for k, line in zip(sequence, lines):
        section = both[:, at : at + len(line)].reshape(len(both), -1)
        found[k] = section[:, : leaves[k].size].reshape(-1, *leaves[k].shape)
        at += len(line)
    numbers = iter(range(len(leaves)))
    return jax.tree.map(lambda _: found[next(numbers)], shard)


def combined_by_axis(shard, axes, combine):
    for axis in axes:
        pieces = collected_together(shard, axis)
        shard = jax.tree.map(lambda part: part[0], pieces)
        for k in range(1, lax.axis_size(axis)):
            shard = combine(shard, jax.tree.map(lambda part: part[k], pieces))
    return shard


def ancestry(parents):
    columns = jnp.arange(PROPS, dtype=jnp.int32)
    parent_link = (parents[:, :, None] == columns[None, None, :]).astype(jnp.float32)
    reached = jnp.eye(PROPS, dtype=jnp.float32)[None] + parent_link
    for squaring in range(PROPS.bit_length()):
        reached = jnp.minimum(jnp.einsum("bij,bjk->bik", reached, reached), 1.0)
    return reached


def combine(earlier, later):
    max_one, sum_one, val_one = earlier
    max_two, sum_two, val_two = later
    joint = jnp.maximum(max_one, max_two)
    factor_one = jnp.exp(max_one - joint)
    factor_two = jnp.exp(max_two - joint)
    return (
        joint,
        factor_one * sum_one + factor_two * sum_two,
        factor_one[..., None] * val_one + factor_two[..., None] * val_two,
    )


def shards(
    tokens,
    norm_gain,
    w_query,
    w_key,
    w_value,
    w_gate,
    gate_bias,
    w_out,
    keys_cache,
    values_cache,
    cum_gates,
    prior_len,
    accepted,
    parents,
):
    row_count = tokens.shape[0]
    column_count = tokens.shape[1]
    seq_count = keys_cache.shape[0]
    length = keys_cache.shape[1]
    head_width = w_query.shape[1]
    head_count = head_width // HEAD
    kv_index = lax.axis_index(KV)
    tp_index = lax.axis_index("tp")
    floats = tokens.astype(jnp.float32)
    square_part = jnp.sum(floats * floats, axis=1)
    scaled = (floats * norm_gain).astype(jnp.bfloat16)
    gate_rows = lax.dynamic_slice_in_dim(w_gate, kv_index * column_count, column_count, 0)
    gate_cols = lax.dynamic_slice_in_dim(gate_rows, tp_index * head_count, head_count, 1)
    gate_part = jnp.dot(scaled, gate_cols, preferred_element_type=jnp.float32)
    bias_local = lax.dynamic_slice_in_dim(gate_bias, tp_index * head_count, head_count, 0)
    gate_sum, square_sum = in_one((gate_part, square_part), KV)
    inv_rms = lax.rsqrt(square_sum / D + norm_eps)
    row_share = row_count // lax.axis_size(KV)
    summed = summed_on_arrival(
        jnp.concatenate(
            [
                jnp.dot(scaled, w_query, preferred_element_type=jnp.float32),
                jnp.dot(scaled, w_key, preferred_element_type=jnp.float32),
                jnp.dot(scaled, w_value, preferred_element_type=jnp.float32),
            ],
            axis=1,
        ).astype(jnp.bfloat16),
        KV,
        0,
    )
    own_rms = lax.dynamic_slice_in_dim(inv_rms, kv_index * row_share, row_share, 0)
    rounded = (own_rms[:, None] * summed).astype(jnp.bfloat16)
    joined = collect(rounded, KV, 0)
    queries = joined[:, :head_width]
    new_keys = joined[:, head_width : 2 * head_width]
    new_values = joined[:, 2 * head_width :]
    log_gates = jax.nn.log_sigmoid(inv_rms[:, None] * gate_sum + bias_local).reshape(
        seq_count, PROPS, head_count
    )
    reached = ancestry(parents)
    tree_gates = jnp.einsum("bij,bjh->bih", reached, log_gates)
    filled = prior_len + accepted
    offset = kv_index * length
    local_last = filled - 1 - offset
    owner_mask = (local_last >= 0) & (local_last < length)
    index_last = jnp.broadcast_to(
        jnp.clip(local_last, 0, length - 1)[:, None, None], (seq_count, head_count, 1)
    )
    last_gate = jnp.take_along_axis(cum_gates, index_last, axis=2)[:, :, 0]
    prop_cum = last_gate[:, None, :] + tree_gates
    scale = HEAD ** (-0.5)
    query_four = queries.reshape(seq_count, PROPS, head_count, HEAD)
    keys_four = keys_cache.reshape(seq_count, length, head_count, HEAD)
    values_four = values_cache.reshape(seq_count, length, head_count, HEAD)
    newk_four = new_keys.reshape(seq_count, PROPS, head_count, HEAD)
    newv_four = new_values.reshape(seq_count, PROPS, head_count, HEAD)
    positions = offset + jnp.arange(length, dtype=jnp.int32)
    valid_keys = positions[None, :] < filled[:, None]
    scores = (
        jnp.einsum("bihd,bphd->bhip", query_four, keys_four, preferred_element_type=jnp.float32)
        * scale
    )
    scores = jnp.where(
        valid_keys[:, None, None, :], scores - cum_gates[:, :, None, :], masked_score
    )
    tree_scores = (
        jnp.einsum("bihd,bjhd->bhij", query_four, newk_four, preferred_element_type=jnp.float32)
        * scale
    )
    tree_scores = tree_scores - jnp.transpose(prop_cum, (0, 2, 1))[:, :, None, :]
    tree_live = (reached > 0.5)[:, None, :, :] & owner_mask[:, None, None, None]
    tree_scores = jnp.where(tree_live, tree_scores, masked_score)
    local_max = jnp.maximum(jnp.max(scores, axis=3), jnp.max(tree_scores, axis=3))
    weights = jnp.where(valid_keys[:, None, None, :], jnp.exp(scores - local_max[..., None]), 0.0)
    tree_weights = jnp.where(tree_live, jnp.exp(tree_scores - local_max[..., None]), 0.0)
    local_sum = jnp.sum(weights, axis=3) + jnp.sum(tree_weights, axis=3)
    local_values = jnp.einsum(
        "bhip,bphd->bhid",
        weights.astype(jnp.bfloat16),
        values_four,
        preferred_element_type=jnp.float32,
    )
    local_values = local_values + jnp.einsum(
        "bhij,bjhd->bhid",
        tree_weights.astype(jnp.bfloat16),
        newv_four,
        preferred_element_type=jnp.float32,
    )
    local_values = lax.optimization_barrier(local_values.astype(jnp.bfloat16)).astype(jnp.float32)
    top_score, grand_total, weighted = combined_by_axis(
        (local_max, local_sum, local_values), KV, combine
    )
    result = weighted / grand_total[..., None]
    attended = (
        jnp.transpose(result, (0, 2, 1, 3)).reshape(row_count, head_width).astype(jnp.bfloat16)
    )
    partial_value = jnp.dot(attended, w_out, preferred_element_type=jnp.float32)
    mixed_rows = summed_on_arrival(partial_value.astype(jnp.bfloat16), "tp", 0).astype(jnp.bfloat16)
    slot_index = positions[None, :] - filled[:, None]
    inside = (slot_index >= 0) & (slot_index < PROPS)
    selector = (slot_index[:, :, None] == jnp.arange(PROPS, dtype=jnp.int32)[None, None, :]).astype(
        jnp.bfloat16
    )
    placed_keys = jnp.einsum(
        "bpj,bjc->bpc",
        selector,
        new_keys.reshape(seq_count, PROPS, head_width),
        preferred_element_type=jnp.float32,
    ).astype(jnp.bfloat16)
    placed_values = jnp.einsum(
        "bpj,bjc->bpc",
        selector,
        new_values.reshape(seq_count, PROPS, head_width),
        preferred_element_type=jnp.float32,
    ).astype(jnp.bfloat16)
    keys_out = jnp.where(inside[:, :, None], placed_keys, keys_cache)
    values_out = jnp.where(inside[:, :, None], placed_values, values_cache)
    return (mixed_rows, keys_out, values_out)


def solution(mesh):
    torus = Mesh(mesh.devices.reshape(8, 4, mesh.shape["tp"]), ("kv_0", "kv_1", "tp"))
    in_specs = (
        P(None, KV),
        P(KV),
        P(KV, "tp"),
        P(KV, "tp"),
        P(KV, "tp"),
        P(),
        P(),
        P("tp", KV),
        P(None, KV, "tp"),
        P(None, KV, "tp"),
        P(None, "tp", KV),
        P(),
        P(),
        P(),
    )
    out_specs = (P("tp", KV), P(None, KV, "tp"), P(None, KV, "tp"))
    return jax.shard_map(
        shards, mesh=torus, in_specs=in_specs, out_specs=out_specs, check_vma=False
    )
```

profile of v0, /device:TPU:1, one launch (start us, length us, event | category | flops | bytes accessed | tf_op | source)
XLA Modules:
  0.0 173.0 jit_solution(7093638999539466821)
XLA Ops:
  7.2 0.9 fusion.43
  8.1 1.1 fusion.84
  10.1 11.9 %all-to-all-start = ((f32[32,1,1152]{2,1,0:T(1,128)}), f32[32,1,1152]{2,1,0:T(1,128)S(1)}, u32[]{:S(2)}, u32[]{:S(2)}) async-start(f32[32,1,1152]{2,1,0:T(1,128)} %broadcast_in_dim.65), calls=%async_computation | async-start | bytes 294912 | tf_op jit(solution)/shard_map/all_to_all | solution.py:19
  24.1 1.1 convolution_convert_fusion.2
  26.0 0.8 pad_maximum_fusion
  26.8 1.0 compare_and_fusion
  27.9 3.6 %all-to-all-done = f32[32,1,1152]{2,1,0:T(1,128)S(1)} async-done(((f32[32,1,1152]{2,1,0:T(1,128)}), f32[32,1,1152]{2,1,0:T(1,128)S(1)}, u32[]{:S(2)}, u32[]{:S(2)}) %all-to-all-start) | async-done | bytes 147488 | tf_op jit(solution)/shard_map/all_to_all | solution.py:19
  31.4 5.7 %all-to-all-start.1 = ((bf16[32,12,384]{2,1,0:T(8,128)(2,1)}), bf16[32,12,384]{2,1,0:T(8,128)(2,1)}, u32[]{:S(2)}, u32[]{:S(2)}) async-start(bf16[32,12,384]{2,1,0:T(8,128)(2,1)} %pad_maximum_fusion), calls=%async_computation.1 | async-start | bytes 786432 | tf_op jit(solution)/shard_map/all_to_all | solution.py:44
  37.4 1.3 gather_fusion
  39.1 4.8 %copy.284 = bf16[24,512,128]{1,2,0:T(8,128)(2,1)} copy(bf16[24,512,128]{2,1,0:T(8,128)(2,1)} %param.22) | data formatting | bytes 6291456 | tf_op args[8]
  43.9 2.8 %copy.297 = bf16[24,512,128]{1,2,0:T(8,128)(2,1)} copy(bf16[24,512,128]{2,1,0:T(8,128)(2,1)S(1)} %copy-done.2) | data formatting | bytes 6291456 | tf_op args[9]
  47.0 3.4 %all-to-all-done.1 = bf16[32,12,384]{2,1,0:T(8,128)(2,1)} async-done(((bf16[32,12,384]{2,1,0:T(8,128)(2,1)}), bf16[32,12,384]{2,1,0:T(8,128)(2,1)}, u32[]{:S(2)}, u32[]{:S(2)}) %all-to-all-start.1) | async-done | bytes 294944 | tf_op jit(solution)/shard_map/all_to_all | solution.py:44
  50.4 1.1 convert_reduce_fusion
  51.5 0.8 broadcast_in_dim.66
  52.3 5.7 %all-to-all-start.2 = ((bf16[32,12,384]{2,1,0:T(8,128)(2,1)}), bf16[32,12,384]{2,1,0:T(8,128)(2,1)S(1)}, u32[]{:S(2)}, u32[]{:S(2)}) async-start(bf16[32,12,384]{2,1,0:T(8,128)(2,1)} %broadcast_in_dim.66), calls=%async_computation.2 | async-start | bytes 786432 | tf_op jit(solution)/shard_map/all_to_all | solution.py:19
  59.1 11.5 %all-to-all-done.2 = bf16[32,12,384]{2,1,0:T(8,128)(2,1)S(1)} async-done(((bf16[32,12,384]{2,1,0:T(8,128)(2,1)}), bf16[32,12,384]{2,1,0:T(8,128)(2,1)S(1)}, u32[]{:S(2)}, u32[]{:S(2)}) %all-to-all-start.2) | async-done | bytes 294944 | tf_op jit(solution)/shard_map/all_to_all | solution.py:19
  71.8 2.6 %fusion.99 = (f32[24,2,16]{2,1,0:T(2,128)S(1)}, f32[24,2,16,512]{3,2,1,0:T(8,128)S(1)}) fusion(f32[24,2,512]{2,1,0:T(2,128)S(1)} %copy-done.1, bf16[24,512,2,64]{1,3,2,0:T(8,128)(2,1)} %bitcast.362, bf16[24,16,2,64]{3,2,1,0:T(2,128)(2,1)S(1)} %reshape.917, pred[24,512]{1,0:T(8,128)(4,1)S(1)} %get-tuple-element.91), kind=kOutput, calls=%fused_computation.196 | convolution fusion | flops 51903744 | bytes 4930560 | tf_op jit(solution)/shard_map/bihd,bphd->bhip/dot_general | solution.py:182
  75.9 2.9 %fusion.2 = bf16[24,2,16,64]{3,2,1,0:T(8,128)(2,1)S(1)} fusion(f32[24,2,16,64]{3,2,1,0:T(8,128)S(1)} %fusion.31, bf16[24,512,2,64]{1,3,2,0:T(8,128)(2,1)} %bitcast.361, f32[24,2,16,512]{3,2,1,0:T(8,128)S(1)} %get-tuple-element.93, f32[24,2,16]{2,1,0:T(2,128)S(1)} %max.309, pred[24,512]{1,0:T(8,128)(4,1)S(1)} %get-tuple-element.91), kind=kOutput, calls=%fused_computation.8 | convolution fusion | flops 51609600 | bytes 5028864 | tf_op jit(solution)/shard_map/bhip,bphd->bhid/dot_general | solution.py:199
  80.3 7.9 %convert_select_fusion = bf16[24,512,128]{2,1,0:T(8,128)(2,1)} fusion(bf16[24,512,128]{2,1,0:T(8,128)(2,1)} %param.23, pred[24,512]{1,0:T(8,128)(4,1)S(1)} %get-tuple-element.90, bf16[24,16,128]{2,1,0:T(8,128)(2,1)S(1)} %bitcast.368, s32[24,512]{1,0:T(8,128)S(1)} %broadcast_subtract_fusion), kind=kOutput, calls=%fused_computation.1 | convolution fusion | flops 53673984 | bytes 6451200 | tf_op jit(solution)/shard_map/bpj,bjc->bpc/dot_general | solution.py:232
  88.2 27.3 %all-gather.6.cloned.1.call-done = f32[8,792,64]{1,2,0:T(8,128)} async-done(((f32[1,792,64]{1,2,0:T(8,128)}), f32[8,792,64]{1,2,0:T(8,128)}) %all-gather.6.cloned.1.call-update) | async-done | bytes 1622032 | tf_op jit(solution)/shard_map/all_gather | solution.py:67
  115.5 1.3 fusion.95
  119.2 12.7 %all-gather.3 = f32[4,792,64]{1,2,0:T(8,128)S(1)} all-gather(f32[1,792,64]{1,2,0:T(8,128)S(1)} %maximum_bitcast_fusion.1), channel_id=3, replica_groups=mesh['kv_0'=8,'kv_1'=4,'tp'=8] {'kv_1'}, dimensions={0}, use_global_device_ids=true | all-gather | bytes 1013760 | tf_op jit(solution)/shard_map/all_gather | solution.py:67
  132.0 0.9 copy.361
  132.9 0.9 copy.362
  133.8 0.9 copy.363
  134.8 0.9 copy.364
  141.2 1.1 multiply_add_fusion
  142.3 2.1 %fusion.37 = bf16[24,16,2,64]{3,1,2,0:T(8,128)(2,1)S(1)} fusion(f32[24,2,16]{2,1,0:T(2,128)S(1)} %bitcast.370, f32[24,2,16,64]{3,2,1,0:T(8,128)} %bitcast.366, f32[24,2,16]{2,1,0:T(2,128)S(1)} %bitcast.376, f32[24,2,16,64]{3,2,1,0:T(8,128)} %bitcast.365, f32[24,2,16]{2,1,0:T(2,128)S(1)} %bitcast.374, f32[24,2,16,64]{3,2,1,0:T(8,128)} %bitcast.364, ...), kind=kLoop, calls=%fused_computation.71 | loop fusion | flops 540672 | bytes 906240 | tf_op jit(solution)/shard_map/convert_element_type | solution.py:217
  144.6 0.8 convert_element_type.70
  145.4 1.1 convolution_convert_fusion.3
  147.3 11.6 %all-to-all-start.3 = ((bf16[8,2,1536]{2,1,0:T(2,128)(2,1)}), bf16[8,2,1536]{2,1,0:T(2,128)(2,1)S(1)}, u32[]{:S(2)}, u32[]{:S(2)}) async-start(bf16[8,2,1536]{2,1,0:T(2,128)(2,1)} %reshape.948), calls=%async_computation.3 | async-start | bytes 98304 | tf_op jit(solution)/shard_map/all_to_all | solution.py:44
  158.9 6.5 %convert_select_fusion.1 = bf16[24,512,128]{2,1,0:T(8,128)(2,1)} fusion(bf16[24,512,128]{2,1,0:T(8,128)(2,1)S(1)} %copy-done.3, pred[24,512]{1,0:T(8,128)(4,1)} %copy-done.6, bf16[24,16,128]{2,1,0:T(8,128)(2,1)S(1)} %bitcast.367, s32[24,512]{1,0:T(8,128)S(1)} %broadcast_subtract_fusion), kind=kOutput, calls=%fused_computation.2 | convolution fusion | flops 53673984 | bytes 6451200 | tf_op jit(solution)/shard_map/bpj,bjc->bpc/dot_general | solution.py:226
  (151 shorter events, 19.6 us)
Async XLA Ops:
  7.2 0.9 copy-start
  7.2 18.1 %copy-start.5 = (bf16[384,64]{0,1:T(8,128)(2,1)S(1)}, bf16[384,64]{0,1:T(8,128)(2,1)}, u32[]{:S(2)}) copy-start(bf16[384,64]{0,1:T(8,128)(2,1)} %param.14) | copy-start | bytes 147460
  7.2 18.1 %copy-start.9 = (f32[64]{0:T(128)S(1)}, f32[64]{0:T(128)}, u32[]{:S(2)}) copy-start(f32[64]{0:T(128)} %param.15) | copy-start | bytes 772
  7.2 18.1 %copy-start.7 = (bf16[64,128]{1,0:T(8,128)(2,1)S(1)}, bf16[64,128]{1,0:T(8,128)(2,1)}, u32[]{:S(2)}) copy-start(bf16[64,128]{1,0:T(8,128)(2,1)} %param.17) | copy-start | bytes 49156
  7.2 18.4 %copy-start.8 = (bf16[64,128]{1,0:T(8,128)(2,1)S(1)}, bf16[64,128]{1,0:T(8,128)(2,1)}, u32[]{:S(2)}) copy-start(bf16[64,128]{1,0:T(8,128)(2,1)} %param.18) | copy-start | bytes 49156
  10.1 21.3 %all-to-all-start = ((f32[32,1,1152]{2,1,0:T(1,128)}), f32[32,1,1152]{2,1,0:T(1,128)S(1)}, u32[]{:S(2)}, u32[]{:S(2)}) async-start(f32[32,1,1152]{2,1,0:T(1,128)} %broadcast_in_dim.65), calls=%async_computation | async-start | bytes 294912 | tf_op jit(solution)/shard_map/all_to_all | solution.py:19
  22.7 24.0 %copy-start.10 = (s32[24]{0:T(128)}, s32[24]{0:T(128)S(1)}, u32[]{:S(2)}) copy-start(s32[24]{0:T(128)S(1)} %get-tuple-element.33) | copy-start | bytes 292
  24.1 13.3 %copy-start.1 = (f32[24,2,512]{2,1,0:T(2,128)S(1)}, f32[24,2,512]{2,1,0:T(2,128)}, u32[]{:S(2)}) copy-start(f32[24,2,512]{2,1,0:T(2,128)} %param.24) | copy-start | bytes 294916
  31.4 18.9 %all-to-all-start.1 = ((bf16[32,12,384]{2,1,0:T(8,128)(2,1)}), bf16[32,12,384]{2,1,0:T(8,128)(2,1)}, u32[]{:S(2)}, u32[]{:S(2)}) async-start(bf16[32,12,384]{2,1,0:T(8,128)(2,1)} %pad_maximum_fusion), calls=%async_computation.1 | async-start | bytes 786432 | tf_op jit(solution)/shard_map/all_to_all | solution.py:44
  37.4 1.4 copy-start.12
  39.1 4.8 %copy-start.2 = (bf16[24,512,128]{2,1,0:T(8,128)(2,1)S(1)}, bf16[24,512,128]{2,1,0:T(8,128)(2,1)}, u32[]{:S(2)}) copy-start(bf16[24,512,128]{2,1,0:T(8,128)(2,1)} %param.23) | copy-start | bytes 9437188
  46.6 12.3 %copy-start.13 = (bf16[24,16,16]{2,1,0:T(8,128)(2,1)S(1)}, bf16[24,16,16]{2,1,0:T(8,128)(2,1)}, u32[]{:S(2)}) copy-start(bf16[24,16,16]{2,1,0:T(8,128)(2,1)} %get-tuple-element.95) | copy-start | bytes 36868
  46.7 33.6 %copy-start.6 = (pred[24,512]{1,0:T(8,128)(4,1)}, pred[24,512]{1,0:T(8,128)(4,1)S(1)}, u32[]{:S(2)}) copy-start(pred[24,512]{1,0:T(8,128)(4,1)S(1)} %get-tuple-element.90) | copy-start | bytes 36868
  52.3 18.3 %all-to-all-start.2 = ((bf16[32,12,384]{2,1,0:T(8,128)(2,1)}), bf16[32,12,384]{2,1,0:T(8,128)(2,1)S(1)}, u32[]{:S(2)}, u32[]{:S(2)}) async-start(bf16[32,12,384]{2,1,0:T(8,128)(2,1)} %broadcast_in_dim.66), calls=%async_computation.2 | async-start | bytes 786432 | tf_op jit(solution)/shard_map/all_to_all | solution.py:19
  58.1 57.4 %all-gather.6.cloned.1.call-start = ((), (), s32[]{:S(2)}) async-start(), calls=%async_computation.4 | async-start | bytes 2064384 | tf_op jit(solution)/shard_map/all_gather | solution.py:67
  78.8 1.4 copy-start.11
  115.5 3.5 %copy-start.4 = (f32[8,792,64]{1,2,0:T(8,128)S(1)}, f32[8,792,64]{1,2,0:T(8,128)}, u32[]{:S(2)}) copy-start(f32[8,792,64]{1,2,0:T(8,128)} %all-gather.6.cloned.1.call-done) | copy-start | bytes 4866052
  140.5 18.5 %copy-start.3 = (bf16[24,512,128]{2,1,0:T(8,128)(2,1)S(1)}, bf16[24,512,128]{2,1,0:T(8,128)(2,1)}, u32[]{:S(2)}) copy-start(bf16[24,512,128]{2,1,0:T(8,128)(2,1)} %param.22) | copy-start | bytes 9437188
  147.3 18.1 %all-to-all-start.3 = ((bf16[8,2,1536]{2,1,0:T(2,128)(2,1)}), bf16[8,2,1536]{2,1,0:T(2,128)(2,1)S(1)}, u32[]{:S(2)}, u32[]{:S(2)}) async-start(bf16[8,2,1536]{2,1,0:T(2,128)(2,1)} %reshape.948), calls=%async_computation.3 | async-start | bytes 98304 | tf_op jit(solution)/shard_map/all_to_all | solution.py:44
Sparse Core Ops, SparseCore 0:
  80.3 35.0 all-gather.5
where the time goes:
time: 174 us; the launch traced here: 173 us
  waiting for transfers between devices  45.9 us (26%)
  starting transfers between devices  35 us (20%)
  local copies, waits for them, and re-layouts  29.2 us (17%)
  matrix products  25.9 us (15%)
  between operations  14.6 us (8%)
  blocking collectives  12.7 us (7%)
  other arithmetic  9.74 us (6%)
    all_gather x1, waiting for transfers between devices, collected_together(): both, at, found = (lax.all_gather(jnp.concatenate(lines), axis), 0, {})  27.3 us
    all_to_all x2, starting transfers between devices, from_everyone(): lax.all_to_all(jnp.broadcast_to(shard[None], (count, *shard.shape)), axis...  17.6 us
    all_to_all x2, starting transfers between devices, summed_on_arrival(): lax.all_to_all(in_blocks(shard, dim, count), axis, 0, 0, tiled=True)  17.4 us
    all_to_all x2, waiting for transfers between devices, from_everyone(): lax.all_to_all(jnp.broadcast_to(shard[None], (count, *shard.shape)), axis...  15.1 us
    unnamed x55, local copies, waits for them, and re-layouts  14.2 us
    all_gather x1, blocking collectives, collected_together(): both, at, found = (lax.all_gather(jnp.concatenate(lines), axis), 0, {})  12.7 us
    dot_general x1, matrix products, shards(): jnp.einsum('bpj,bjc->bpc', selector, new_values.reshape(seq_count, PROPS,...  7.86 us
    dot_general x1, matrix products, shards(): jnp.einsum('bpj,bjc->bpc', selector, new_keys.reshape(seq_count, PROPS, h...  6.47 us
  transfers between devices with their start and end apart: 5, of which 4 were waited for; matrix products, arithmetic and copies ran while one was open for 18% of the time, Pallas kernels for 0%

commit v1 on v0

v1 whole, which is shorter than its diff:
```python
import functools

import jax
import jax.numpy as jnp
from jax import lax
from jax.experimental import pallas as pl
from jax.experimental.pallas import tpu as pltpu
from jax.sharding import PartitionSpec as P

D = 2048
HEAD = 64
PROPS = 16
SEQS = 24
NZ, NX = 8, 4
NKV = NZ * NX
WIDE = 128
MASKED = 1e30
NORM_EPS = 1e-06
FIRST_WRITER = 4

f32, bf16 = jnp.float32, jnp.bfloat16


def iota(shape, dim):
    return lax.broadcasted_iota(jnp.int32, shape, dim)


def dot_nt(a, b):
    return lax.dot_general(a, b, (((1,), (1,)), ((), ())), preferred_element_type=f32)


def dot_nn(a, b):
    return lax.dot_general(a, b, (((1,), (0,)), ((), ())), preferred_element_type=f32)


def far_first(i):
    return 4 + (1 - 2 * lax.rem(i, 2)) * lax.div(i + 1, 2)


def near_first(i):
    odd = lax.rem(i, 2)
    return odd * lax.div(i + 1, 2) + (1 - odd) * lax.rem(NZ - lax.div(i, 2), NZ)


def owner_of(z, r):
    return z * NX + lax.rem(z + 1 + r, NX)


def split_heads(rows):
    lane = iota((2 * PROPS, WIDE), 1)
    sub = iota((2 * PROPS, WIDE), 0)
    both = jnp.concatenate([rows, rows], axis=0)
    return jnp.where((lane < HEAD) == (sub < PROPS), both, 0.0).astype(bf16)


def join_heads(rows):
    lane = iota((PROPS, WIDE), 1)
    return jnp.where(lane < HEAD, rows[:PROPS], rows[PROPS:])


def as_row(tops, sums):
    lane = iota((2 * PROPS, WIDE), 1)
    sub = iota((2 * PROPS, WIDE), 0)
    spread = jnp.where(lane == sub, tops, jnp.where(lane == sub + 2 * PROPS, sums, 0.0))
    return jnp.sum(spread, axis=0, keepdims=True)


def as_column(row, start):
    lane = iota((PROPS, WIDE), 1)
    sub = iota((PROPS, WIDE), 0)
    return jnp.sum(jnp.where(lane == sub + start, row, 0.0), axis=1, keepdims=True)


def step_kernel(
    tp_count,
    tok_hbm,
    gain_hbm,
    wq_hbm,
    wk_hbm,
    wv_hbm,
    wg_hbm,
    wo_hbm,
    keys_hbm,
    values_hbm,
    cum_hbm,
    bias_ref,
    prior_ref,
    accepted_ref,
    parents_ref,
    mixed_ref,
    new_ref,
    tok,
    gain,
    wq,
    wk,
    wv,
    wg,
    wo,
    keys,
    values,
    cum,
    part_q,
    part_n,
    part_s,
    got_q,
    got_n,
    got_s,
    queries,
    own_new,
    out_v,
    out_s,
    got_v,
    got_m,
    attended,
    reach,
    heads_out,
    heads_in,
    local_sems,
    send_sems,
    recv_sems,
    query_sems,
    new_sems,
    att_sems,
):
    me = lax.axis_index("kv")
    tp = lax.axis_index("tp")
    my_z, my_x = lax.div(me, NX), lax.rem(me, NX)
    my_r = lax.rem(my_x - my_z - 1 + 2 * NX * NZ, NX)
    owner = my_r < 3
    own_b = lax.min(3 * my_z + my_r, SEQS - 1)
    length = keys.shape[1]
    offset = me * length
    heads = 2

    barrier = pltpu.get_barrier_semaphore()

    @pl.loop(0, NKV - 1)
    def _(i):
        pl.semaphore_signal(barrier, inc=1, device_id={"kv": lax.rem(me + i + 1, NKV)})

    @pl.loop(0, tp_count - 1)
    def _(i):
        pl.semaphore_signal(barrier, inc=1, device_id={"tp": lax.rem(tp + i + 1, tp_count)})

    gate_block = pl.multiple_of(lax.div(me, 2) * WIDE, WIDE)
    pairs = (
        (tok_hbm, tok),
        (gain_hbm, gain),
        (wg_hbm.at[:, pl.ds(gate_block, WIDE)], wg),
        (wq_hbm, wq),
        (wk_hbm, wk),
        (wv_hbm, wv),
        (cum_hbm, cum),
        (keys_hbm, keys),
        (values_hbm, values),
        (wo_hbm, wo),
    )
    loads = [pltpu.make_async_copy(a, b, local_sems.at[i]) for i, (a, b) in enumerate(pairs)]
    for load in loads:
        load.start()

    @pl.when(owner)
    def _():
        lane = iota((PROPS, WIDE), 1)
        sub = iota((PROPS, WIDE), 0)
        parent = jnp.full((PROPS, WIDE), -1, jnp.int32)
        for j in range(PROPS):
            parent = jnp.where(sub == j, parents_ref[j, own_b], parent)
        seen = jnp.where((lane == sub) | (lane == parent), 1.0, 0.0)
        rest = jnp.zeros((WIDE - PROPS, WIDE), f32)
        for _ in range(4):
            square = jnp.concatenate([seen, rest], axis=0).astype(bf16)
            seen = jnp.minimum(dot_nn(seen.astype(bf16), square), 1.0)
        reach[...] = jnp.concatenate([seen, rest], axis=0)

    for load in loads[:6]:
        load.wait()
    x = tok[...].astype(f32)
    width = x.shape[0]
    eye = iota((width, width), 0) == iota((width, width), 1)
    gain_col = jnp.sum(jnp.where(eye, gain[...], 0.0), axis=1, keepdims=True)
    square_row = jnp.sum(x * x, axis=0, keepdims=True)
    scaled_t = x * gain_col
    scaled = jnp.transpose(scaled_t).astype(bf16)
    gate_w = wg[...].astype(f32)
    gate_w = jnp.where(lax.rem(me, 2) == 0, gate_w[:, :width], gate_w[:, width:]).astype(bf16)
    gates = dot_nn(gate_w, scaled_t.astype(bf16))
    gate_row = iota(gates.shape, 0)
    rows = [square_row] + [
        jnp.sum(jnp.where(gate_row == heads * tp + h, gates, 0.0), axis=0, keepdims=True)
        for h in range(heads)
    ]
    for j in range(3):
        for k, row in enumerate(rows):
            part_s[j, pl.ds(k, 1), :] = row[:, j * WIDE : (j + 1) * WIDE]
        part_s[j, pl.ds(3, 1), :] = jnp.zeros((1, WIDE), f32)
    part_q[...] = dot_nn(scaled, wq[...]).astype(bf16).reshape(SEQS, PROPS, WIDE)
    part_n[:, :, :WIDE] = dot_nn(scaled, wk[...]).astype(bf16).reshape(SEQS, PROPS, WIDE)
    part_n[:, :, WIDE:] = dot_nn(scaled, wv[...]).astype(bf16).reshape(SEQS, PROPS, WIDE)

    pl.semaphore_wait(barrier, NKV - 1 + tp_count - 1)

    def remote(src, dst, send, recv, where):
        return pltpu.make_async_remote_copy(
            src_ref=src, dst_ref=dst, send_sem=send, recv_sem=recv, device_id=where
        )

    def to_owners(body):
        @pl.loop(0, NZ)
        def _(i):
            z = lax.rem(my_z + far_first(i), NZ)
            for r in range(3):
                peer = owner_of(z, r)

                @pl.when(peer != me)
                def _():
                    body(3 * z + r, peer)

    def to_all(low, body):
        @pl.loop(0, NZ)
        def _(i):
            z = lax.rem(my_z + far_first(i), NZ)

            @pl.when(z >= low)
            def _():
                for k in range(NX):
                    x_at = lax.rem(my_x + (2, 1, 3, 0)[k], NX)
                    peer = z * NX + x_at

                    @pl.when(peer != me)
                    def _():
                        body(peer)

    def send_queries(b, peer):
        remote(part_q.at[b], got_q.at[me], send_sems.at[0], recv_sems.at[0], {"kv": peer}).start()
        remote(
            part_s.at[lax.div(b, 8)], got_s.at[me], send_sems.at[1], recv_sems.at[1], {"kv": peer}
        ).start()

    def send_new(b, peer):
        remote(part_n.at[b], got_n.at[me], send_sems.at[2], recv_sems.at[2], {"kv": peer}).start()

    to_owners(send_queries)
    to_owners(send_new)

    def all_arrived(ref, sem):
        most = ref.at[pl.ds(0, NKV - 1)]
        pltpu.make_async_copy(most, most, sem).wait()

    def own_inverse(sums, at):
        return lax.rsqrt(as_column(sums[0:1], at) / D + NORM_EPS)

    own_lane = lax.rem(own_b, 8) * PROPS

    @pl.when(owner)
    def _():
        got_q[me] = part_q[own_b]
        got_n[me] = part_n[own_b]
        got_s[me] = part_s[lax.div(own_b, 8)]
        all_arrived(got_s, recv_sems.at[1])
        all_arrived(got_q, recv_sems.at[0])
        sums = jnp.sum(got_s[...], axis=0)
        inverse = own_inverse(sums, own_lane)
        total = jnp.sum(got_q[...].astype(f32), axis=0)
        rounded = (inverse * total).astype(bf16).astype(f32)
        queries[own_b] = (rounded * HEAD**-0.5).astype(bf16)

        def send(peer):
            remote(
                queries.at[own_b],
                queries.at[own_b],
                send_sems.at[3],
                query_sems.at[own_b],
                {"kv": peer},
            ).start()

        to_all(0, send)

    for load in loads[6:9]:
        load.wait()
    positions = offset + iota((1, length), 1)

    @pl.loop(0, NZ)
    def _(i):
        z = lax.rem(my_z + near_first(i), NZ)
        for r in range(3):
            b = 3 * z + r
            peer = owner_of(z, r)

            @pl.when(peer != me)
            def _():
                mine = queries.at[b]
                pltpu.make_async_copy(mine, mine, query_sems.at[b]).wait()

        for r in range(3):
            b = 3 * z + r
            filled = prior_ref[b] + accepted_ref[b]
            gates_b = cum[b]
            last = jnp.sum(
                jnp.where(positions == filled - 1, gates_b, 0.0), axis=1, keepdims=True
            )
            bias = jnp.where(positions < filled, gates_b, MASKED)
            bias = jnp.concatenate(
                [jnp.broadcast_to(bias[h : h + 1], (PROPS, length)) for h in range(heads)], axis=0
            )
            scores = dot_nt(split_heads(queries[b].astype(f32)), keys[b]) - bias
            top = jnp.max(scores, axis=1, keepdims=True)
            weights = jnp.exp(scores - top)
            total = jnp.sum(weights, axis=1, keepdims=True)
            out_v[b] = join_heads(dot_nn(weights.astype(bf16), values[b])).astype(bf16)
            lane = iota((1, WIDE), 1)
            row = as_row(top, total)
            row = row + jnp.where(lane == 64, last[0:1], 0.0) + jnp.where(lane == 65, last[1:2], 0.0)
            out_s[b] = row

        for r in range(3):
            b = 3 * z + r
            peer = owner_of(z, r)

            @pl.when(peer != me)
            def _():
                remote(
                    out_s.at[b], got_m.at[me], send_sems.at[4], recv_sems.at[3], {"kv": peer}
                ).start()
                remote(
                    out_v.at[b], got_v.at[me], send_sems.at[5], recv_sems.at[4], {"kv": peer}
                ).start()

    @pl.when(owner)
    def _():
        got_v[me] = out_v[own_b]
        got_m[me] = out_s[own_b]

        all_arrived(got_n, recv_sems.at[2])
        sums = jnp.sum(got_s[...], axis=0)
        inverse = own_inverse(sums, own_lane)
        new = (inverse * jnp.sum(got_n[...].astype(f32), axis=0)).astype(bf16)
        own_new[...] = new

        def send(peer):
            remote(
                own_new, new_ref.at[own_b], send_sems.at[6], new_sems.at[own_b], {"kv": peer}
            ).start()

        to_all(FIRST_WRITER, send)

        seen = reach[...]
        seen_t = jnp.transpose(seen)[:PROPS]
        bias_rows = []
        for h in range(heads):
            logit = inverse * as_column(sums[h + 1 : h + 2], own_lane) + bias_ref[heads * tp + h]
            log_gate = jnp.minimum(logit, 0.0) - jnp.log1p(jnp.exp(-jnp.abs(logit)))
            tree_gate = jnp.sum(seen_t * log_gate, axis=0, keepdims=True)
            bias_rows.append(jnp.broadcast_to(tree_gate, (PROPS, WIDE)))
        rest = jnp.zeros((WIDE - PROPS, WIDE), bf16)
        new_keys = jnp.concatenate([new[:, :WIDE], rest], axis=0)
        new_values = jnp.concatenate([new[:, WIDE:], rest], axis=0)
        live = jnp.concatenate([seen[:PROPS], seen[:PROPS]], axis=0) > 0.5
        scores = dot_nt(split_heads(queries[own_b].astype(f32)), new_keys)
        scores = jnp.where(live, scores - jnp.concatenate(bias_rows, axis=0), -MASKED)
        top = jnp.max(scores, axis=1, keepdims=True)
        weights = jnp.where(live, jnp.exp(scores - top), 0.0)
        total = jnp.sum(weights, axis=1, keepdims=True)
        got_v[NKV] = join_heads(dot_nn(weights.astype(bf16), new_values)).astype(bf16)
        tree_row = as_row(top, total)

        all_arrived(got_m, recv_sems.at[3])
        lane = iota((1, WIDE), 1)
        stats = got_m[pl.ds(0, NKV)]
        ends = jnp.sum(stats, axis=0)
        last_0 = jnp.sum(jnp.where(lane == 64, ends, 0.0), axis=1, keepdims=True)
        last_1 = jnp.sum(jnp.where(lane == 65, ends, 0.0), axis=1, keepdims=True)
        shift = jnp.where(lane < PROPS, last_0, jnp.where(lane < 2 * PROPS, last_1, 0.0))
        got_m[NKV] = tree_row - shift
        stats = got_m[...]
        top = jnp.max(stats, axis=0, keepdims=True)
        held = lane.reshape(1, 1, WIDE) < 2 * PROPS
        factors = jnp.exp(jnp.where(held, stats - top, 0.0))
        sums_in = jnp.concatenate([stats[:, :, 32:], stats[:, :, :32]], axis=2)
        grand = jnp.sum(factors * sums_in, axis=0, keepdims=True)
        shares = factors / jnp.where(held, grand, 1.0)
        all_arrived(got_v, recv_sems.at[4])
        first = iota((PROPS, WIDE), 1) < HEAD
        result = jnp.zeros((PROPS, WIDE), f32)
        for s in range(NKV + 1):
            share = shares[s]
            pair = jnp.where(first, as_column(share, 0), as_column(share, PROPS))
            result = result + pair * got_v[s].astype(f32)
        attended[own_b] = result.astype(bf16)

        def send_rows(peer):
            remote(
                attended.at[own_b],
                attended.at[own_b],
                send_sems.at[7],
                att_sems.at[own_b],
                {"kv": peer},
            ).start()

        to_all(0, send_rows)

    loads[9].wait()
    per = NZ // tp_count

    @pl.loop(0, NZ)
    def _(i):
        z = lax.rem(my_z + near_first(i), NZ)
        for r in range(3):
            b = 3 * z + r
            peer = owner_of(z, r)

            @pl.when(peer != me)
            def _():
                mine = attended.at[b]
                pltpu.make_async_copy(mine, mine, att_sems.at[b]).wait()

        rows_in = attended[pl.ds(3 * z, 3)].reshape(3 * PROPS, WIDE)
        heads_out[z] = dot_nt(rows_in, wo[...]).astype(bf16)
        to, part = lax.div(z, per), lax.rem(z, per)

        @pl.when(to == tp)
        def _():
            heads_in[tp * per + part] = heads_out[z]

        @pl.when(to != tp)
        def _():
            remote(
                heads_out.at[z],
                heads_in.at[tp * per + part],
                send_sems.at[8],
                recv_sems.at[5],
                {"tp": to},
            ).start()

    def sent(ref, count, sem):
        some = ref.at[pl.ds(0, count)]
        pltpu.make_async_copy(some, some, sem).wait()

    if tp_count > 1:
        sent(heads_in, NZ - per, recv_sems.at[5])
    for part in range(per):
        total = heads_in[part].astype(f32)
        for s in range(1, tp_count):
            total = total + heads_in[s * per + part].astype(f32)
        mixed_ref[pl.ds(part * 3 * PROPS, 3 * PROPS), :] = total.astype(bf16)

    @pl.when(my_z >= FIRST_WRITER)
    def _():
        @pl.when(owner)
        def _():
            copy = pltpu.make_async_copy(own_new, new_ref.at[own_b], local_sems.at[10])
            copy.start()
            copy.wait()

        @pl.loop(0, NZ)
        def _(z):
            for r in range(3):

                @pl.when(owner_of(z, r) != me)
                def _():
                    there = new_ref.at[3 * z + r]
                    pltpu.make_async_copy(there, there, new_sems.at[3 * z + r]).wait()

    def sent_to_owners(count):
        sent(part_q, count, send_sems.at[0])
        sent(got_s, count, send_sems.at[1])
        sent(part_n, count, send_sems.at[2])
        sent(out_s, count, send_sems.at[4])
        sent(out_v, count, send_sems.at[5])

    @pl.when(owner)
    def _():
        sent_to_owners(SEQS - 1)
        sent(got_v, NKV - 1, send_sems.at[3])
        sent(got_v, NKV - 1, send_sems.at[7])
        writers = NKV - NX * FIRST_WRITER

        @pl.when(my_z >= FIRST_WRITER)
        def _():
            sent(part_n, writers - 1, send_sems.at[6])

        @pl.when(my_z < FIRST_WRITER)
        def _():
            sent(part_n, writers, send_sems.at[6])

    @pl.when(jnp.logical_not(owner))
    def _():
        sent_to_owners(SEQS)

    if tp_count > 1:
        sent(heads_out, NZ - per, send_sems.at[8])


def write_kernel(
    mixed_in, new_ref, prior_ref, accepted_ref, keys_hbm, values_hbm,
    mixed_out, keys_out, values_out,
    keys, values, sems_in, sems_out,
):
    me = lax.axis_index("kv")
    length = keys.shape[1]
    both = ((keys_hbm, keys, keys_out), (values_hbm, values, values_out))

    def copy_in(k, b):
        return pltpu.make_async_copy(both[k][0].at[b], both[k][1].at[b], sems_in.at[k, b])

    def copy_out(k, b):
        return pltpu.make_async_copy(both[k][1].at[b], both[k][2].at[b], sems_out.at[k, b])

    @pl.loop(0, SEQS)
    def _(b):
        for k in range(2):
            copy_in(k, b).start()

    mixed_out[...] = mixed_in[...]

    @pl.loop(0, SEQS)
    def _(b):
        start = prior_ref[b] + accepted_ref[b] - me * length
        touched = (start > -PROPS) & (start < length)
        for k in range(2):
            copy_in(k, b).wait()

        @pl.when(touched)
        def _():
            base = jnp.clip(lax.shift_right_arithmetic(start, 4), 0, length // PROPS - 2) * PROPS
            rows = pl.ds(pl.multiple_of(base, PROPS), 2 * PROPS)
            slot = iota((2 * PROPS, PROPS), 0) + (base - start)
            pick = jnp.where(slot == iota((2 * PROPS, PROPS), 1), 1.0, 0.0).astype(bf16)
            placed = dot_nn(pick, new_ref[b])
            at = iota((2 * PROPS, WIDE), 0) + (base - start)
            inside = (at >= 0) & (at < PROPS)
            for k in range(2):
                held = both[k][1]
                old = held[b, rows, :].astype(f32)
                fresh = placed[:, k * WIDE : (k + 1) * WIDE]
                held[b, rows, :] = jnp.where(inside, fresh, old).astype(bf16)

        for k in range(2):
            copy_out(k, b).start()

    @pl.loop(0, SEQS)
    def _(b):
        for k in range(2):
            copy_out(k, b).wait()


def shards(
    tokens, norm_gain, w_query, w_key, w_value, w_gate, gate_bias, w_out,
    keys_cache, values_cache, cum_gates, prior_len, accepted, parents,
):
    tp_count = lax.axis_size("tp")
    rows, width = tokens.shape
    columns = w_out.shape[1]
    length = keys_cache.shape[1]
    any_ = pl.BlockSpec(memory_space=pl.ANY)
    smem = pl.BlockSpec(memory_space=pltpu.SMEM)
    vmem = pl.BlockSpec(memory_space=pltpu.VMEM)
    out_rows = rows // tp_count
    dma = pltpu.SemaphoreType.DMA
    mixed, new = pl.pallas_call(
        functools.partial(step_kernel, tp_count),
        out_shape=(
            jax.ShapeDtypeStruct((out_rows, columns), bf16),
            jax.ShapeDtypeStruct((SEQS, PROPS, 2 * WIDE), bf16),
        ),
        in_specs=[any_] * 10 + [smem] * 4,
        out_specs=(vmem, any_),
        scratch_shapes=[
            pltpu.VMEM((width, rows), bf16),
            pltpu.VMEM((1, width), f32),
            pltpu.VMEM((width, WIDE), bf16),
            pltpu.VMEM((width, WIDE), bf16),
            pltpu.VMEM((width, WIDE), bf16),
            pltpu.VMEM((w_gate.shape[1], WIDE), bf16),
            pltpu.VMEM((columns, WIDE), bf16),
            pltpu.VMEM(keys_cache.shape, bf16),
            pltpu.VMEM(values_cache.shape, bf16),
            pltpu.VMEM(cum_gates.shape, f32),
            pltpu.VMEM((SEQS, PROPS, WIDE), bf16),
            pltpu.VMEM((SEQS, PROPS, 2 * WIDE), bf16),
            pltpu.VMEM((3, 4, WIDE), f32),
            pltpu.VMEM((NKV, PROPS, WIDE), bf16),
            pltpu.VMEM((NKV, PROPS, 2 * WIDE), bf16),
            pltpu.VMEM((NKV, 4, WIDE), f32),
            pltpu.VMEM((SEQS, PROPS, WIDE), bf16),
            pltpu.VMEM((PROPS, 2 * WIDE), bf16),
            pltpu.VMEM((SEQS, PROPS, WIDE), bf16),
            pltpu.VMEM((SEQS, 1, WIDE), f32),
            pltpu.VMEM((NKV + 1, PROPS, WIDE), bf16),
            pltpu.VMEM((NKV + 1, 1, WIDE), f32),
            pltpu.VMEM((SEQS, PROPS, WIDE), bf16),
            pltpu.VMEM((WIDE, WIDE), f32),
            pltpu.VMEM((NZ, 3 * PROPS, columns), bf16),
            pltpu.VMEM((NZ, 3 * PROPS, columns), bf16),
            dma((11,)),
            dma((9,)),
            dma((6,)),
            dma((SEQS,)),
            dma((SEQS,)),
            dma((SEQS,)),
        ],
        compiler_params=pltpu.CompilerParams(collective_id=0, has_side_effects=True),
        name="tree_step",
    )(
        tokens.T, norm_gain.reshape(1, width), w_query, w_key, w_value, w_gate.T, w_out.T,
        keys_cache, values_cache, cum_gates, gate_bias, prior_len, accepted, parents.T,
    )
    return pl.pallas_call(
        write_kernel,
        out_shape=(
            jax.ShapeDtypeStruct((out_rows, columns), bf16),
            jax.ShapeDtypeStruct(keys_cache.shape, bf16),
            jax.ShapeDtypeStruct(values_cache.shape, bf16),
        ),
        in_specs=[vmem, vmem, smem, smem, any_, any_],
        out_specs=(vmem, any_, any_),
        scratch_shapes=[
            pltpu.VMEM(keys_cache.shape, bf16),
            pltpu.VMEM(values_cache.shape, bf16),
            dma((2, SEQS)),
            dma((2, SEQS)),
        ],
        name="cache_write",
    )(mixed, new, prior_len, accepted, keys_cache, values_cache)


def solution(mesh):
    in_specs = (
        P(None, "kv"),
        P("kv"),
        P("kv", "tp"),
        P("kv", "tp"),
        P("kv", "tp"),
        P(),
        P(),
        P("tp", "kv"),
        P(None, "kv", "tp"),
        P(None, "kv", "tp"),
        P(None, "tp", "kv"),
        P(),
        P(),
        P(),
    )
    out_specs = (P("tp", "kv"), P(None, "kv", "tp"), P(None, "kv", "tp"))
    return jax.shard_map(
        shards, mesh=mesh, in_specs=in_specs, out_specs=out_specs, check_vma=False
    )
```

time: 174 us -> 56.3 us (0.32)
  Pallas kernels: 0 us -> 55.4 us
  waiting for transfers between devices: 45.9 us -> 0 us
  starting transfers between devices: 35 us -> 0 us
  local copies, waits for them, and re-layouts: 29.2 us -> 0 us
  matrix products: 25.9 us -> 0 us
  between operations: 14.6 us -> 0.64 us
  blocking collectives: 12.7 us -> 0 us
  other arithmetic: 9.74 us -> 0 us
    pallas_call x0 -> x2, Pallas kernels: none -> 55.4 us  [the longest x1 47.9 us: shards(): pl.pallas_call(functools.partial(step_kernel, tp_count), out_shape=(jax.S...]
    all_to_all x4 -> x0, starting transfers between devices: 35 us -> none  [the longest x2 17.6 us: from_everyone(): lax.all_to_all(jnp.broadcast_to(shard[None], (count, *shard.shape)), axis...]
    all_gather x1 -> x0, waiting for transfers between devices: 27.3 us -> none  [collected_together(): both, at, found = (lax.all_gather(jnp.concatenate(lines), axis), 0, {})]
    dot_general x15 -> x0, matrix products: 25.9 us -> none  [the longest x1 7.86 us: shards(): jnp.einsum('bpj,bjc->bpc', selector, new_values.reshape(seq_count, PROPS,...]
    all_to_all x4 -> x0, waiting for transfers between devices: 18.6 us -> none  [the longest x2 15.1 us: from_everyone(): lax.all_to_all(jnp.broadcast_to(shard[None], (count, *shard.shape)), axis...]
    unnamed x55 -> x0, local copies, waits for them, and re-layouts: 14.2 us -> none
    all_gather x1 -> x0, blocking collectives: 12.7 us -> none  [collected_together(): both, at, found = (lax.all_gather(jnp.concatenate(lines), axis), 0, {})]
    squeeze x16 -> x0, local copies, waits for them, and re-layouts: 5.55 us -> none  [the longest x13 4.08 us: combined_by_axis(): shard = combine(shard, jax.tree.map(lambda part: part[k], pieces))]
  transfers between devices with their start and end apart: 5 -> 0, of which waited for: 4 -> 0; matrix products, arithmetic and copies ran while one was open for 18% -> 0% of each run, Pallas kernels for 0% -> 0%
where the time goes in v1:
time: 56.3 us; the launch traced here: 56 us
  Pallas kernels  55.4 us (98%)
  between operations  0.64 us (1%)
    pallas_call x1, Pallas kernels, shards(): pl.pallas_call(functools.partial(step_kernel, tp_count), out_shape=(jax.S...  47.9 us
    pallas_call x1, Pallas kernels, shards(): pl.pallas_call(write_kernel, out_shape=(jax.ShapeDtypeStruct((out_rows, c...  7.52 us

profile of v1, /device:TPU:1, one launch (start us, length us, event | category | flops | bytes accessed | tf_op | source)
XLA Modules:
  0.0 56.0 jit_solution(12577580808433611339)
XLA Ops:
  0.6 47.9 %tree_step.1 = (bf16[48,64]{1,0:T(8,128)(2,1)}, bf16[24,16,256]{2,1,0:T(8,128)(2,1)}) custom-call(bf16[64,384]{1,0:T(8,128)(2,1)} %bitcast.6, f32[1,64]{1,0:T(1,128)} %bitcast.9, bf16[64,128]{1,0:T(8,128)(2,1)} %wq_hbm.1, bf16[64,128]{1,0:T(8,128)(2,1)} %wk_hbm.1, bf16[64,128]{1,0:T(8,128)(2,1)} %wv_hbm.1, bf16[16,2048]{1,0:T(8,128)(2,1)} %bitcast.5, ...), custom_call_target="tpu_custom_call" | custom-call | tf_op jit(solution)/shard_map/tree_step/pallas_call | solution.py:560
  48.5 7.5 %cache_write.1 = (bf16[48,64]{1,0:T(8,128)(2,1)}, bf16[24,512,128]{2,1,0:T(8,128)(2,1)}, bf16[24,512,128]{2,1,0:T(8,128)(2,1)}) custom-call(bf16[48,64]{1,0:T(8,128)(2,1)} %get-tuple-element.5.mixed_in, bf16[24,16,256]{2,1,0:T(8,128)(2,1)} %get-tuple-element.6.new_ref, s32[24]{0:T(128)} %prior_ref.3, s32[24]{0:T(128)} %accepted_ref.3, ...), custom_call_target="tpu_custom_call" | custom-call | tf_op jit(solution)/shard_map/cache_write/pallas_call | solution.py:608

commit v2 on v1

v2 whole, which is shorter than its diff:
```python
import functools

import jax
import jax.numpy as jnp
from jax import lax
from jax.experimental import pallas as pl
from jax.experimental.pallas import tpu as pltpu
from jax.sharding import PartitionSpec as P

D = 2048
HEAD = 64
PROPS = 16
SEQS = 24
NZ, NX = 8, 4
NKV = NZ * NX
WIDE = 128
MASKED = 1e30
NORM_EPS = 1e-06
FIRST_WRITER = 4

f32, bf16 = jnp.float32, jnp.bfloat16


def iota(shape, dim):
    return lax.broadcasted_iota(jnp.int32, shape, dim)


def dot_nt(a, b):
    return lax.dot_general(a, b, (((1,), (1,)), ((), ())), preferred_element_type=f32)


def dot_nn(a, b):
    return lax.dot_general(a, b, (((1,), (0,)), ((), ())), preferred_element_type=f32)


def far_first(i):
    return 4 + (1 - 2 * lax.rem(i, 2)) * lax.div(i + 1, 2)


def near_first(i):
    odd = lax.rem(i, 2)
    return odd * lax.div(i + 1, 2) + (1 - odd) * lax.rem(NZ - lax.div(i, 2), NZ)


def owner_of(z, r):
    return z * NX + lax.rem(z + 1 + r, NX)


def split_heads(rows):
    lane = iota((2 * PROPS, WIDE), 1)
    sub = iota((2 * PROPS, WIDE), 0)
    both = jnp.concatenate([rows, rows], axis=0)
    return jnp.where((lane < HEAD) == (sub < PROPS), both, 0.0).astype(bf16)


def join_heads(rows):
    lane = iota((PROPS, WIDE), 1)
    return jnp.where(lane < HEAD, rows[:PROPS], rows[PROPS:])


def as_row(tops, sums):
    lane = iota((2 * PROPS, WIDE), 1)
    sub = iota((2 * PROPS, WIDE), 0)
    spread = jnp.where(lane == sub, tops, jnp.where(lane == sub + 2 * PROPS, sums, 0.0))
    return jnp.sum(spread, axis=0, keepdims=True)


def as_column(row, start):
    lane = iota((PROPS, WIDE), 1)
    sub = iota((PROPS, WIDE), 0)
    return jnp.sum(jnp.where(lane == sub + start, row, 0.0), axis=1, keepdims=True)


def step_kernel(
    tp_count,
    tok_hbm,
    gain_hbm,
    wq_hbm,
    wk_hbm,
    wv_hbm,
    wg_hbm,
    wo_hbm,
    keys_hbm,
    values_hbm,
    cum_hbm,
    bias_hbm,
    prior_hbm,
    accepted_hbm,
    parents_hbm,
    mixed_ref,
    new_ref,
    keys,
    values,
    bias_ref,
    prior_ref,
    accepted_ref,
    parents_ref,
    tok,
    gain,
    wq,
    wk,
    wv,
    wg,
    wo,
    keys_t,
    cum,
    part_q,
    part_n,
    part_s,
    got_q,
    got_n,
    got_s,
    queries,
    own_new,
    out_v,
    out_s,
    got_v,
    got_m,
    own_rows,
    got_rows,
    reach,
    local_sems,
    send_sems,
    recv_sems,
    query_sems,
    new_sems,
    planes_in,
):
    me = lax.axis_index("kv")
    tp = lax.axis_index("tp")
    my_z, my_x = lax.div(me, NX), lax.rem(me, NX)
    my_r = lax.rem(my_x - my_z - 1 + 2 * NX * NZ, NX)
    owner = my_r < 3
    own_b = lax.min(my_z + NZ * my_r, SEQS - 1)
    per = SEQS // tp_count
    own_to = lax.div(own_b, per)
    length = keys.shape[1]
    offset = me * length
    heads = 2

    barrier = pltpu.get_barrier_semaphore()

    @pl.loop(0, NKV - 1)
    def _(i):
        pl.semaphore_signal(barrier, inc=1, device_id={"kv": lax.rem(me + i + 1, NKV)})

    @pl.loop(0, tp_count - 1)
    def _(i):
        pl.semaphore_signal(barrier, inc=1, device_id={"tp": lax.rem(tp + i + 1, tp_count)})

    gate_block = pl.multiple_of(lax.div(me, 2) * WIDE, WIDE)
    pairs = (
        (parents_hbm, parents_ref),
        (bias_hbm, bias_ref),
        (prior_hbm, prior_ref),
        (accepted_hbm, accepted_ref),
        (tok_hbm, tok),
        (gain_hbm, gain),
        (wg_hbm.at[:, pl.ds(gate_block, WIDE)], wg),
        (wq_hbm, wq),
        (wk_hbm, wk),
        (wv_hbm, wv),
        (cum_hbm, cum),
        (keys_hbm, keys),
        (values_hbm, values),
        (wo_hbm, wo.at[tp]),
    )
    loads = [pltpu.make_async_copy(a, b, local_sems.at[i]) for i, (a, b) in enumerate(pairs)]
    for load in loads:
        load.start()

    loads[0].wait()

    @pl.when(owner)
    def _():
        lane = iota((PROPS, WIDE), 1)
        sub = iota((PROPS, WIDE), 0)
        parent = jnp.full((PROPS, WIDE), -1, jnp.int32)
        for j in range(PROPS):
            parent = jnp.where(sub == j, parents_ref[j, own_b], parent)
        seen = jnp.where((lane == sub) | (lane == parent), 1.0, 0.0)
        rest = jnp.zeros((WIDE - PROPS, WIDE), f32)
        for _ in range(4):
            square = jnp.concatenate([seen, rest], axis=0).astype(bf16)
            seen = jnp.minimum(dot_nn(seen.astype(bf16), square), 1.0)
        reach[...] = jnp.concatenate([seen, rest], axis=0)

    with jax.named_scope("wait_inputs"):
        for load in loads[4:10]:
            load.wait()
    x = tok[...].astype(f32)
    width = x.shape[0]
    eye = iota((width, width), 0) == iota((width, width), 1)
    gain_col = jnp.sum(jnp.where(eye, gain[...], 0.0), axis=1, keepdims=True)
    square_row = jnp.sum(x * x, axis=0, keepdims=True)
    scaled_t = x * gain_col
    scaled = jnp.transpose(scaled_t).astype(bf16)
    gate_w = wg[...].astype(f32)
    gate_w = jnp.where(lax.rem(me, 2) == 0, gate_w[:, :width], gate_w[:, width:]).astype(bf16)
    gates = dot_nn(gate_w, scaled_t.astype(bf16))
    gate_row = iota(gates.shape, 0)
    rows = [square_row] + [
        jnp.sum(jnp.where(gate_row == heads * tp + h, gates, 0.0), axis=0, keepdims=True)
        for h in range(heads)
    ]
    sub, lane = iota((8, WIDE), 0), iota((8, WIDE), 1)
    for j in range(3):
        tile = jnp.zeros((8, WIDE), f32)
        for k, row in enumerate(rows):
            part = row[:, j * WIDE : (j + 1) * WIDE]
            part = pltpu.roll(jnp.broadcast_to(part, (8, WIDE)), k * PROPS, 1)
            tile = jnp.where(sub == k, part, tile)
        for c in range(8):
            moved = pltpu.roll(tile, (WIDE - c * PROPS) % WIDE, 1)
            moved = jnp.where(lax.shift_right_logical(lane, 4) == sub, moved, 0.0)
            part_s[8 * j + c] = jnp.sum(moved, axis=0, keepdims=True)
    part_q[...] = dot_nn(scaled, wq[...]).astype(bf16).reshape(SEQS, PROPS, WIDE)
    part_n[:, :, :WIDE] = dot_nn(scaled, wk[...]).astype(bf16).reshape(SEQS, PROPS, WIDE)
    part_n[:, :, WIDE:] = dot_nn(scaled, wv[...]).astype(bf16).reshape(SEQS, PROPS, WIDE)

    with jax.named_scope("barrier"):
        pl.semaphore_wait(barrier, NKV - 1 + tp_count - 1)

    def remote(src, dst, send, recv, where):
        return pltpu.make_async_remote_copy(
            src_ref=src, dst_ref=dst, send_sem=send, recv_sem=recv, device_id=where
        )

    def to_owners(body):
        @pl.loop(0, NZ)
        def _(i):
            z = lax.rem(my_z + far_first(i), NZ)
            for r in range(3):
                peer = owner_of(z, r)

                @pl.when(peer != me)
                def _():
                    body(z + NZ * r, peer)

    def to_everyone(low, body):
        @pl.loop(0, NZ)
        def _(i):
            z = lax.rem(my_z + far_first(i), NZ)

            @pl.when(z >= low)
            def _():
                for k in range(NX):
                    body(z * NX + lax.rem(my_x + (2, 1, 3, 0)[k], NX))

    def to_all(low, body):
        def other(peer):
            @pl.when(peer != me)
            def _():
                body(peer)

        to_everyone(low, other)

    def send_queries(b, peer):
        remote(part_q.at[b], got_q.at[me], send_sems.at[0], recv_sems.at[0], {"kv": peer}).start()
        remote(part_s.at[b], got_s.at[me], send_sems.at[1], recv_sems.at[1], {"kv": peer}).start()

    def send_new(b, peer):
        remote(part_n.at[b], got_n.at[me], send_sems.at[2], recv_sems.at[2], {"kv": peer}).start()

    with jax.named_scope("send_parts"):
        to_owners(send_queries)

    loads[13].wait()

    @pl.loop(0, tp_count - 1)
    def _(i):
        there = {"tp": lax.rem(tp + i + 1, tp_count)}
        pl.semaphore_signal(planes_in, inc=1, device_id=there)
        remote(wo.at[tp], wo.at[tp], send_sems.at[8], recv_sems.at[5], there).start()

    with jax.named_scope("wait_cache"):
        for load in (loads[1], loads[2], loads[3], loads[10], loads[11]):
            load.wait()
    positions = offset + iota((1, length), 1)

    with jax.named_scope("prepare"):

        @pl.loop(0, SEQS)
        def _(b):
            filled = prior_ref[b] + accepted_ref[b]
            gates_b = cum[b]
            last = jnp.sum(
                jnp.where(positions == filled - 1, gates_b, 0.0), axis=1, keepdims=True
            )
            cum[b] = jnp.where(positions < filled, gates_b, MASKED)
            lane = iota((1, WIDE), 1)
            row = jnp.where(lane == 64, last[0:1], 0.0) + jnp.where(lane == 65, last[1:2], 0.0)
            out_s[b] = row
            keys_t[b] = jnp.transpose(keys[b])

    def all_arrived(ref, sem):
        most = ref.at[pl.ds(0, NKV - 1)]
        pltpu.make_async_copy(most, most, sem).wait()

    def own_inverse(sums):
        return lax.rsqrt(as_column(sums, 0) / D + NORM_EPS)

    @pl.when(owner)
    def _():
        got_q[me] = part_q[own_b]
        got_n[me] = part_n[own_b]
        got_s[me] = part_s[own_b]
        with jax.named_scope("wait_parts"):
            all_arrived(got_s, recv_sems.at[1])
            all_arrived(got_q, recv_sems.at[0])
        sums = jnp.sum(got_s[...], axis=0)
        inverse = own_inverse(sums)
        total = jnp.sum(got_q[...].astype(f32), axis=0)
        rounded = (inverse * total).astype(bf16).astype(f32)
        queries[own_b] = (rounded * HEAD**-0.5).astype(bf16)

        def send(peer):
            remote(
                queries.at[own_b],
                queries.at[own_b],
                send_sems.at[3],
                query_sems.at[own_b],
                {"kv": peer},
            ).start()

        with jax.named_scope("send_queries"):
            to_all(0, send)

    with jax.named_scope("send_new"):
        to_owners(send_new)

    with jax.named_scope("wait_cache"):
        loads[12].wait()

    @pl.loop(0, NZ)
    def _(i):
        z = lax.rem(my_z + near_first(i), NZ)
        for r in range(3):
            b = z + NZ * r
            peer = owner_of(z, r)

            @pl.when(peer != me)
            def _():
                with jax.named_scope("wait_query"):
                    mine = queries.at[b]
                    pltpu.make_async_copy(mine, mine, query_sems.at[b]).wait()

        group = range(3)
        scores = []
        for r in group:
            bias = cum[z + NZ * r]
            bias = jnp.concatenate(
                [jnp.broadcast_to(bias[h : h + 1], (PROPS, length)) for h in range(heads)], axis=0
            )
            query = split_heads(queries[z + NZ * r].astype(f32))
            scores.append(dot_nn(query, keys_t[z + NZ * r]) - bias)
        tops = [jnp.max(scores[r], axis=1, keepdims=True) for r in group]
        weights = [jnp.exp(scores[r] - tops[r]) for r in group]
        totals = [jnp.sum(weights[r], axis=1, keepdims=True) for r in group]
        blocks = [dot_nn(weights[r].astype(bf16), values[z + NZ * r]) for r in group]
        for r in group:
            out_s[z + NZ * r] = out_s[z + NZ * r] + as_row(tops[r], totals[r])
            out_v[z + NZ * r] = join_heads(blocks[r]).astype(bf16)

        for r in range(3):
            b = z + NZ * r
            peer = owner_of(z, r)

            @pl.when(peer != me)
            def _():
                remote(
                    out_s.at[b], got_m.at[me], send_sems.at[4], recv_sems.at[3], {"kv": peer}
                ).start()
                remote(
                    out_v.at[b], got_v.at[me], send_sems.at[5], recv_sems.at[4], {"kv": peer}
                ).start()

    @pl.when(owner)
    def _():
        got_v[me] = out_v[own_b]
        got_m[me] = out_s[own_b]

        with jax.named_scope("wait_new"):
            all_arrived(got_n, recv_sems.at[2])
        sums = jnp.sum(got_s[...], axis=0)
        inverse = own_inverse(sums)
        new = (inverse * jnp.sum(got_n[...].astype(f32), axis=0)).astype(bf16)
        own_new[...] = new

        def send(peer):
            remote(
                own_new, new_ref.at[own_b], send_sems.at[6], new_sems.at[own_b], {"kv": peer}
            ).start()

        to_all(FIRST_WRITER, send)

        seen = reach[...]
        seen_t = jnp.transpose(seen)[:PROPS]
        bias_rows = []
        for h in range(heads):
            logit = inverse * as_column(sums, PROPS * (h + 1)) + bias_ref[heads * tp + h]
            log_gate = jnp.minimum(logit, 0.0) - jnp.log1p(jnp.exp(-jnp.abs(logit)))
            tree_gate = jnp.sum(seen_t * log_gate, axis=0, keepdims=True)
            bias_rows.append(jnp.broadcast_to(tree_gate, (PROPS, WIDE)))
        rest = jnp.zeros((WIDE - PROPS, WIDE), bf16)
        new_keys = jnp.concatenate([new[:, :WIDE], rest], axis=0)
        new_values = jnp.concatenate([new[:, WIDE:], rest], axis=0)
        live = jnp.concatenate([seen[:PROPS], seen[:PROPS]], axis=0) > 0.5
        scores = dot_nt(split_heads(queries[own_b].astype(f32)), new_keys)
        scores = jnp.where(live, scores - jnp.concatenate(bias_rows, axis=0), -MASKED)
        top = jnp.max(scores, axis=1, keepdims=True)
        weights = jnp.where(live, jnp.exp(scores - top), 0.0)
        total = jnp.sum(weights, axis=1, keepdims=True)
        got_v[NKV] = join_heads(dot_nn(weights.astype(bf16), new_values)).astype(bf16)
        tree_row = as_row(top, total)

        with jax.named_scope("wait_stats"):
            all_arrived(got_m, recv_sems.at[3])
        lane = iota((1, WIDE), 1)
        stats = got_m[pl.ds(0, NKV)]
        ends = jnp.sum(stats, axis=0)
        last_0 = jnp.sum(jnp.where(lane == 64, ends, 0.0), axis=1, keepdims=True)
        last_1 = jnp.sum(jnp.where(lane == 65, ends, 0.0), axis=1, keepdims=True)
        shift = jnp.where(lane < PROPS, last_0, jnp.where(lane < 2 * PROPS, last_1, 0.0))
        got_m[NKV] = tree_row - shift
        stats = got_m[...]
        top = jnp.max(stats, axis=0, keepdims=True)
        held = lane.reshape(1, 1, WIDE) < 2 * PROPS
        factors = jnp.exp(jnp.where(held, stats - top, 0.0))
        sums_in = jnp.concatenate([stats[:, :, 32:], stats[:, :, :32]], axis=2)
        grand = jnp.sum(factors * sums_in, axis=0, keepdims=True)
        shares = factors / jnp.where(held, grand, 1.0)
        with jax.named_scope("wait_blocks"):
            all_arrived(got_v, recv_sems.at[4])
        first = iota((PROPS, WIDE), 1) < HEAD
        result = jnp.zeros((PROPS, WIDE), f32)
        for s in range(NKV + 1):
            share = shares[s]
            pair = jnp.where(first, as_column(share, 0), as_column(share, PROPS))
            result = result + pair * got_v[s].astype(f32)
        own_rows[...] = result.astype(bf16)
        slot = lax.rem(own_b, per)

        if tp_count > 1:
            pl.semaphore_wait(planes_in, tp_count - 1)

        def send_rows(peer):
            @pl.when(jnp.logical_or(peer != me, own_to != tp))
            def _():
                remote(
                    own_rows,
                    got_rows.at[tp, slot],
                    send_sems.at[7],
                    recv_sems.at[6],
                    {"kv": peer, "tp": own_to},
                ).start()

        with jax.named_scope("send_rows"):
            to_everyone(0, send_rows)

        @pl.when(own_to == tp)
        def _():
            got_rows[tp, slot] = own_rows[...]

    def arrived(ref, count, sem):
        some = ref.at[pl.ds(0, count)]
        pltpu.make_async_copy(some, some, sem).wait()

    sent = arrived
    if tp_count > 1:
        arrived(wo, tp_count - 1, recv_sems.at[5])

    with jax.named_scope("wait_rows"):
        mine_too = jnp.logical_and(owner, own_to == tp)

        @pl.when(mine_too)
        def _():
            arrived(got_v, tp_count * per - 1, recv_sems.at[6])

        @pl.when(jnp.logical_not(mine_too))
        def _():
            arrived(got_v, tp_count * per, recv_sems.at[6])

    total = jnp.zeros((per * PROPS, wo.shape[1]), f32)
    for s in range(tp_count):
        rows_in = got_rows[s].reshape(per * PROPS, WIDE)
        total = total + dot_nt(rows_in, wo[s]).astype(bf16).astype(f32)
    mixed_ref[...] = total.astype(bf16)

    @pl.when(my_z >= FIRST_WRITER)
    def _():
        @pl.when(owner)
        def _():
            copy = pltpu.make_async_copy(own_new, new_ref.at[own_b], local_sems.at[14])
            copy.start()
            copy.wait()

        @pl.loop(0, NZ)
        def _(z):
            for r in range(3):

                @pl.when(owner_of(z, r) != me)
                @jax.named_scope("wait_fresh")
                def _():
                    there = new_ref.at[z + NZ * r]
                    pltpu.make_async_copy(there, there, new_sems.at[z + NZ * r]).wait()

    def sent_to_owners(count):
        sent(part_q, count, send_sems.at[0])
        sent(got_s, count, send_sems.at[1])
        sent(part_n, count, send_sems.at[2])
        sent(out_s, count, send_sems.at[4])
        sent(out_v, count, send_sems.at[5])

    @pl.when(owner)
    def _():
        sent_to_owners(SEQS - 1)
        sent(got_v, NKV - 1, send_sems.at[3])

        @pl.when(own_to == tp)
        def _():
            sent(got_v, NKV - 1, send_sems.at[7])

        @pl.when(own_to != tp)
        def _():
            sent(got_v, NKV, send_sems.at[7])

        writers = NKV - NX * FIRST_WRITER

        @pl.when(my_z >= FIRST_WRITER)
        def _():
            sent(part_n, writers - 1, send_sems.at[6])

        @pl.when(my_z < FIRST_WRITER)
        def _():
            sent(part_n, writers, send_sems.at[6])

    @pl.when(jnp.logical_not(owner))
    def _():
        sent_to_owners(SEQS)

    if tp_count > 1:

        @pl.when(jnp.logical_not(owner))
        def _():
            pl.semaphore_wait(planes_in, tp_count - 1)

        sent(wo, tp_count - 1, send_sems.at[8])


def write_kernel(
    mixed_in, new_ref, prior_ref, accepted_ref, keys, values,
    mixed_out, keys_out, values_out, sems_out, sem_mixed,
):
    me = lax.axis_index("kv")
    length = keys.shape[1]
    both = ((keys, keys_out), (values, values_out))

    def copy_out(k, b):
        return pltpu.make_async_copy(both[k][0].at[b], both[k][1].at[b], sems_out.at[k, b])

    mixed = pltpu.make_async_copy(mixed_in, mixed_out, sem_mixed)
    mixed.start()

    @pl.loop(0, SEQS)
    def _(b):
        start = prior_ref[b] + accepted_ref[b] - me * length

        @pl.when((start > -PROPS) & (start < length))
        def _():
            base = jnp.clip(lax.shift_right_arithmetic(start, 4), 0, length // PROPS - 2) * PROPS
            rows = pl.ds(pl.multiple_of(base, PROPS), 2 * PROPS)
            slot = iota((2 * PROPS, PROPS), 0) + (base - start)
            pick = jnp.where(slot == iota((2 * PROPS, PROPS), 1), 1.0, 0.0).astype(bf16)
            placed = dot_nn(pick, new_ref[b])
            at = iota((2 * PROPS, WIDE), 0) + (base - start)
            inside = (at >= 0) & (at < PROPS)
            for k in range(2):
                held = both[k][0]
                old = held[b, rows, :].astype(f32)
                fresh = placed[:, k * WIDE : (k + 1) * WIDE]
                held[b, rows, :] = jnp.where(inside, fresh, old).astype(bf16)

        for k in range(2):
            copy_out(k, b).start()

    @pl.loop(0, SEQS)
    def _(b):
        for k in range(2):
            copy_out(k, b).wait()

    mixed.wait()


def on_chip(shape, dtype):
    return pltpu.VMEM(shape, dtype)


def shards(
    tokens, norm_gain, w_query, w_key, w_value, w_gate, gate_bias, w_out,
    keys_cache, values_cache, cum_gates, prior_len, accepted, parents,
):
    tp_count = lax.axis_size("tp")
    rows, width = tokens.shape
    columns = w_out.shape[1]
    length = keys_cache.shape[1]
    any_ = pl.BlockSpec(memory_space=pl.ANY)
    smem = pl.BlockSpec(memory_space=pltpu.SMEM)
    vmem = pl.BlockSpec(memory_space=pltpu.VMEM)
    out_rows = rows // tp_count
    dma = pltpu.SemaphoreType.DMA
    mixed, new, keys_held, values_held = pl.pallas_call(
        functools.partial(step_kernel, tp_count),
        out_shape=(
            on_chip((out_rows, columns), bf16),
            on_chip((SEQS, PROPS, 2 * WIDE), bf16),
            on_chip(keys_cache.shape, bf16),
            on_chip(values_cache.shape, bf16),
        ),
        in_specs=[pl.BlockSpec(memory_space=pltpu.HBM)] * 14,
        out_specs=(vmem, vmem, vmem, vmem),
        scratch_shapes=[
            pltpu.SMEM(gate_bias.shape, f32),
            pltpu.SMEM(prior_len.shape, jnp.int32),
            pltpu.SMEM(accepted.shape, jnp.int32),
            pltpu.SMEM(parents.shape[::-1], jnp.int32),
            pltpu.VMEM((width, rows), bf16),
            pltpu.VMEM((1, width), f32),
            pltpu.VMEM((width, WIDE), bf16),
            pltpu.VMEM((width, WIDE), bf16),
            pltpu.VMEM((width, WIDE), bf16),
            pltpu.VMEM((w_gate.shape[1], WIDE), bf16),
            pltpu.VMEM((tp_count, columns, WIDE), bf16),
            pltpu.VMEM((SEQS, WIDE, length), bf16),
            pltpu.VMEM(cum_gates.shape, f32),
            pltpu.VMEM((SEQS, PROPS, WIDE), bf16),
            pltpu.VMEM((SEQS, PROPS, 2 * WIDE), bf16),
            pltpu.VMEM((SEQS, 1, WIDE), f32),
            pltpu.VMEM((NKV, PROPS, WIDE), bf16),
            pltpu.VMEM((NKV, PROPS, 2 * WIDE), bf16),
            pltpu.VMEM((NKV, 1, WIDE), f32),
            pltpu.VMEM((SEQS, PROPS, WIDE), bf16),
            pltpu.VMEM((PROPS, 2 * WIDE), bf16),
            pltpu.VMEM((SEQS, PROPS, WIDE), bf16),
            pltpu.VMEM((SEQS, 1, WIDE), f32),
            pltpu.VMEM((NKV + 1, PROPS, WIDE), bf16),
            pltpu.VMEM((NKV + 1, 1, WIDE), f32),
            pltpu.VMEM((PROPS, WIDE), bf16),
            pltpu.VMEM((tp_count, SEQS // tp_count, PROPS, WIDE), bf16),
            pltpu.VMEM((WIDE, WIDE), f32),
            dma((15,)),
            dma((9,)),
            dma((7,)),
            dma((SEQS,)),
            dma((SEQS,)),
            pltpu.SemaphoreType.REGULAR,
        ],
        compiler_params=pltpu.CompilerParams(
            collective_id=0, has_side_effects=True, vmem_limit_bytes=24 << 20
        ),
        name="tree_step",
    )(
        *(
            pltpu.with_memory_space_constraint(x, pltpu.HBM)
            for x in (
                tokens.T, norm_gain.reshape(1, width), w_query, w_key, w_value, w_gate.T, w_out.T,
                keys_cache, values_cache, cum_gates, gate_bias, prior_len, accepted, parents.T,
            )
        )
    )

    def held(x):
        return pltpu.with_memory_space_constraint(x, pltpu.VMEM)

    return pl.pallas_call(
        write_kernel,
        out_shape=(
            jax.ShapeDtypeStruct((out_rows, columns), bf16),
            jax.ShapeDtypeStruct(keys_cache.shape, bf16),
            jax.ShapeDtypeStruct(values_cache.shape, bf16),
        ),
        in_specs=[vmem, vmem, smem, smem, vmem, vmem],
        out_specs=(any_, any_, any_),
        scratch_shapes=[dma((2, SEQS)), dma],
        compiler_params=pltpu.CompilerParams(vmem_limit_bytes=8 << 20),
        name="cache_write",
    )(held(mixed), held(new), prior_len, accepted, held(keys_held), held(values_held))


def solution(mesh):
    in_specs = (
        P(None, "kv"),
        P("kv"),
        P("kv", "tp"),
        P("kv", "tp"),
        P("kv", "tp"),
        P(),
        P(),
        P("tp", "kv"),
        P(None, "kv", "tp"),
        P(None, "kv", "tp"),
        P(None, "tp", "kv"),
        P(),
        P(),
        P(),
    )
    out_specs = (P("tp", "kv"), P(None, "kv", "tp"), P(None, "kv", "tp"))
    return jax.shard_map(
        shards, mesh=mesh, in_specs=in_specs, out_specs=out_specs, check_vma=False
    )
```

time: 56.3 us -> 44.9 us (0.80)
  Pallas kernels: 55.4 us -> 44.2 us
    pallas_call x1, Pallas kernels: 47.9 us -> 40.6 us  [shards(): pl.pallas_call(functools.partial(step_kernel, tp_count), out_shape=(on_ch...]
    pallas_call x1, Pallas kernels: 7.52 us -> 3.61 us  [shards(): pl.pallas_call(write_kernel, out_shape=(jax.ShapeDtypeStruct((out_rows, c...]
where the time goes in v2:
time: 44.9 us
  Pallas kernels  44.2 us (98%)
  between operations  0.68 us (2%)
    pallas_call x1, Pallas kernels, shards(): pl.pallas_call(functools.partial(step_kernel, tp_count), out_shape=(on_ch...  40.6 us
    pallas_call x1, Pallas kernels, shards(): pl.pallas_call(write_kernel, out_shape=(jax.ShapeDtypeStruct((out_rows, c...  3.61 us

profile of v2, /device:TPU:1, one launch (start us, length us, event | category | flops | bytes accessed | tf_op | source)
XLA Modules:
  0.0 44.9 jit_solution(16913901950160312533)
XLA Ops:
  0.6 0.0 copy-start
  0.6 0.0 copy-start.1
  0.7 40.6 %tree_step.1 = (bf16[48,64]{1,0:T(8,128)(2,1)S(1)}, bf16[24,16,256]{2,1,0:T(8,128)(2,1)S(1)}, bf16[24,512,128]{2,1,0:T(8,128)(2,1)S(1)}, bf16[24,512,128]{2,1,0:T(8,128)(2,1)S(1)}) custom-call(bf16[64,384]{1,0:T(8,128)(2,1)} %bitcast.6, f32[1,64]{1,0:T(1,128)} %bitcast.9, bf16[64,128]{1,0:T(8,128)(2,1)} %wq_hbm.1, bf16[64,128]{1,0:T(8,128)(2,1)} %wk_hbm.1, ...), custom_call_target="tpu_custom_call" | custom-call | tf_op jit(solution)/shard_map/tree_step/pallas_call | solution.py:612
  41.2 0.0 copy-done
  41.2 0.0 copy-done.1
  41.2 3.6 %cache_write.1 = (bf16[48,64]{1,0:T(8,128)(2,1)}, bf16[24,512,128]{2,1,0:T(8,128)(2,1)}, bf16[24,512,128]{2,1,0:T(8,128)(2,1)}) custom-call(bf16[48,64]{1,0:T(8,128)(2,1)S(1)} %get-tuple-element.7.mixed_in, bf16[24,16,256]{2,1,0:T(8,128)(2,1)S(1)} %get-tuple-element.8.new_ref, s32[24]{0:T(128)S(1)} %copy-done, s32[24]{0:T(128)S(1)} %copy-done.1, ...), custom_call_target="tpu_custom_call" | custom-call | tf_op jit(solution)/shard_map/cache_write/pallas_call | solution.py:675
Async XLA Ops:
  0.6 40.6 %copy-start = (s32[24]{0:T(128)S(1)}, s32[24]{0:T(128)}, u32[]{:S(2)}) copy-start(s32[24]{0:T(128)} %prior_ref.1) | copy-start | bytes 292
  0.6 40.6 %copy-start.1 = (s32[24]{0:T(128)S(1)}, s32[24]{0:T(128)}, u32[]{:S(2)}) copy-start(s32[24]{0:T(128)} %accepted_ref.1) | copy-start | bytes 292

commit v3 on v2

--- a/solution.py
+++ b/solution.py
@@ -108,6 +108,8 @@
     part_n,
     part_s,
     got_q,
+    got_x,
+    sum_x,
     got_n,
     got_s,
     queries,
@@ -123,7 +125,7 @@
     send_sems,
     recv_sems,
     query_sems,
-    new_sems,
+    row_sems,
     planes_in,
 ):
     me = lax.axis_index("kv")
@@ -140,9 +142,15 @@
 
     barrier = pltpu.get_barrier_semaphore()
 
-    @pl.loop(0, NKV - 1)
+    @pl.loop(0, NZ)
     def _(i):
-        pl.semaphore_signal(barrier, inc=1, device_id={"kv": lax.rem(me + i + 1, NKV)})
+        z = lax.rem(my_z + far_first(i), NZ)
+        for k in range(NX):
+            peer = z * NX + lax.rem(my_x + (2, 1, 3, 0)[k], NX)
+
+            @pl.when(peer != me)
+            def _():
+                pl.semaphore_signal(barrier, inc=1, device_id={"kv": peer})
 
     @pl.loop(0, tp_count - 1)
     def _(i):
@@ -259,8 +267,51 @@
         remote(part_q.at[b], got_q.at[me], send_sems.at[0], recv_sems.at[0], {"kv": peer}).start()
         remote(part_s.at[b], got_s.at[me], send_sems.at[1], recv_sems.at[1], {"kv": peer}).start()
 
-    def send_new(b, peer):
-        remote(part_n.at[b], got_n.at[me], send_sems.at[2], recv_sems.at[2], {"kv": peer}).start()
+    def along_x(body):
+        @pl.loop(0, NZ)
+        def _(z):
+            for r in range(3):
+                body(z + NZ * r, z, lax.rem(z + 1 + r, NX))
+
+    def in_column(body):
+        @pl.loop(0, NZ)
+        def _(i):
+            z = lax.rem(my_z + far_first(i), NZ)
+            r = lax.rem(my_x - z - 1 + 2 * NX * NZ, NX)
+
+            @pl.when(r < 3)
+            def _():
+                body(lax.min(z + NZ * r, SEQS - 1), z)
+
+    def send_new(b, z, x_at):
+        slot = NX * z + my_x
+
+        @pl.when(x_at != my_x)
+        def _():
+            there = {"kv": my_z * NX + x_at}
+            remote(
+                part_n.at[b], got_x.at[slot], send_sems.at[2], recv_sems.at[2], there
+            ).start()
+
+        @pl.when(x_at == my_x)
+        def _():
+            got_x[slot] = part_n[b]
+
+    def pass_new(b, z):
+        total = jnp.sum(got_x[pl.ds(NX * z, NX)].astype(f32), axis=0)
+        sum_x[z] = total.astype(bf16)
+
+    def send_sums(b, z):
+        @pl.when(z != my_z)
+        def _():
+            there = {"kv": z * NX + my_x}
+            remote(
+                sum_x.at[z], got_n.at[my_z], send_sems.at[9], recv_sems.at[3], there
+            ).start()
+
+        @pl.when(z == my_z)
+        def _():
+            got_n[my_z] = sum_x[z]
 
     with jax.named_scope("send_parts"):
         to_owners(send_queries)
@@ -272,6 +323,8 @@
         there = {"tp": lax.rem(tp + i + 1, tp_count)}
         pl.semaphore_signal(planes_in, inc=1, device_id=there)
         remote(wo.at[tp], wo.at[tp], send_sems.at[8], recv_sems.at[5], there).start()
+
+    along_x(send_new)
 
     with jax.named_scope("wait_cache"):
         for load in (loads[1], loads[2], loads[3], loads[10], loads[11]):
@@ -293,9 +346,14 @@
             out_s[b] = row
             keys_t[b] = jnp.transpose(keys[b])
 
+    def arrived(ref, count, sem):
+        some = ref.at[pl.ds(0, count)]
+        pltpu.make_async_copy(some, some, sem).wait()
+
+    sent = arrived
+
     def all_arrived(ref, sem):
-        most = ref.at[pl.ds(0, NKV - 1)]
-        pltpu.make_async_copy(most, most, sem).wait()
+        arrived(ref, NKV - 1, sem)
 
     def own_inverse(sums):
         return lax.rsqrt(as_column(sums, 0) / D + NORM_EPS)
@@ -303,7 +361,6 @@
     @pl.when(owner)
     def _():
         got_q[me] = part_q[own_b]
-        got_n[me] = part_n[own_b]
         got_s[me] = part_s[own_b]
         with jax.named_scope("wait_parts"):
             all_arrived(got_s, recv_sems.at[1])
@@ -319,60 +376,63 @@
                 queries.at[own_b],
                 queries.at[own_b],
                 send_sems.at[3],
-                query_sems.at[own_b],
+                query_sems.at[my_z],
                 {"kv": peer},
             ).start()
 
         with jax.named_scope("send_queries"):
             to_all(0, send)
 
-    with jax.named_scope("send_new"):
-        to_owners(send_new)
+    with jax.named_scope("pass_new"):
+        arrived(got_x, SEQS - SEQS // NX, recv_sems.at[2])
+        in_column(pass_new)
+        in_column(send_sums)
 
     with jax.named_scope("wait_cache"):
         loads[12].wait()
 
-    @pl.loop(0, NZ)
+    @pl.loop(0, NZ // 2)
     def _(i):
-        z = lax.rem(my_z + near_first(i), NZ)
-        for r in range(3):
-            b = z + NZ * r
-            peer = owner_of(z, r)
-
-            @pl.when(peer != me)
-            def _():
-                with jax.named_scope("wait_query"):
-                    mine = queries.at[b]
-                    pltpu.make_async_copy(mine, mine, query_sems.at[b]).wait()
-
-        group = range(3)
+        pair = [lax.rem(my_z + near_first(2 * i + k), NZ) for k in range(2)]
+        for z in pair:
+            with jax.named_scope("wait_query"):
+                mine_too = jnp.logical_and(owner, z == my_z)
+
+                @pl.when(mine_too)
+                def _():
+                    arrived(queries, 2, query_sems.at[z])
+
+                @pl.when(jnp.logical_not(mine_too))
+                def _():
+                    arrived(queries, 3, query_sems.at[z])
+
+        group = [(z + NZ * r, owner_of(z, r)) for z in pair for r in range(3)]
         scores = []
-        for r in group:
-            bias = cum[z + NZ * r]
+        for b, _ in group:
+            bias = cum[b]
             bias = jnp.concatenate(
                 [jnp.broadcast_to(bias[h : h + 1], (PROPS, length)) for h in range(heads)], axis=0
             )
-            query = split_heads(queries[z + NZ * r].astype(f32))
-            scores.append(dot_nn(query, keys_t[z + NZ * r]) - bias)
-        tops = [jnp.max(scores[r], axis=1, keepdims=True) for r in group]
-        weights = [jnp.exp(scores[r] - tops[r]) for r in group]
-        totals = [jnp.sum(weights[r], axis=1, keepdims=True) for r in group]
-        blocks = [dot_nn(weights[r].astype(bf16), values[z + NZ * r]) for r in group]
-        for r in group:
-            out_s[z + NZ * r] = out_s[z + NZ * r] + as_row(tops[r], totals[r])
-            out_v[z + NZ * r] = join_heads(blocks[r]).astype(bf16)
-
-        for r in range(3):
-            b = z + NZ * r
-            peer = owner_of(z, r)
+            query = split_heads(queries[b].astype(f32))
+            scores.append(dot_nn(query, keys_t[b]) - bias)
+        tops = [jnp.max(x, axis=1, keepdims=True) for x in scores]
+        weights = [jnp.exp(x - top) for x, top in zip(scores, tops)]
+        totals = [jnp.sum(x, axis=1, keepdims=True) for x in weights]
+        blocks = [dot_nn(x.astype(bf16), values[b]) for x, (b, _) in zip(weights, group)]
+        for k, (b, _) in enumerate(group):
+            out_s[b] = out_s[b] + as_row(tops[k], totals[k])
+            out_v[b] = join_heads(blocks[k]).astype(bf16)
+
+        for b, peer in group:
 
             @pl.when(peer != me)
             def _():
+                there = {"kv": peer}
                 remote(
-                    out_s.at[b], got_m.at[me], send_sems.at[4], recv_sems.at[3], {"kv": peer}
+                    out_s.at[b], got_m.at[me], send_sems.at[4], recv_sems.at[7], there
                 ).start()
                 remote(
-                    out_v.at[b], got_v.at[me], send_sems.at[5], recv_sems.at[4], {"kv": peer}
+                    out_v.at[b], got_v.at[me], send_sems.at[5], recv_sems.at[4], there
                 ).start()
 
     @pl.when(owner)
@@ -381,18 +441,24 @@
         got_m[me] = out_s[own_b]
 
         with jax.named_scope("wait_new"):
-            all_arrived(got_n, recv_sems.at[2])
+            arrived(got_n, NZ - 1, recv_sems.at[3])
         sums = jnp.sum(got_s[...], axis=0)
         inverse = own_inverse(sums)
         new = (inverse * jnp.sum(got_n[...].astype(f32), axis=0)).astype(bf16)
         own_new[...] = new
 
-        def send(peer):
-            remote(
-                own_new, new_ref.at[own_b], send_sems.at[6], new_sems.at[own_b], {"kv": peer}
-            ).start()
-
-        to_all(FIRST_WRITER, send)
+        for k in range(FIRST_WRITER, NZ):
+
+            @pl.when(my_z != k)
+            def _():
+                there = {"kv": k * NX + my_x}
+                remote(
+                    own_new, new_ref.at[own_b], send_sems.at[6], recv_sems.at[6], there
+                ).start()
+
+        @pl.when(my_z >= FIRST_WRITER)
+        def _():
+            new_ref[own_b] = new
 
         seen = reach[...]
         seen_t = jnp.transpose(seen)[:PROPS]
@@ -415,7 +481,7 @@
         tree_row = as_row(top, total)
 
         with jax.named_scope("wait_stats"):
-            all_arrived(got_m, recv_sems.at[3])
+            all_arrived(got_m, recv_sems.at[7])
         lane = iota((1, WIDE), 1)
         stats = got_m[pl.ds(0, NKV)]
         ends = jnp.sum(stats, axis=0)
@@ -451,7 +517,7 @@
                     own_rows,
                     got_rows.at[tp, slot],
                     send_sems.at[7],
-                    recv_sems.at[6],
+                    row_sems.at[tp],
                     {"kv": peer, "tp": own_to},
                 ).start()
 
@@ -462,55 +528,35 @@
         def _():
             got_rows[tp, slot] = own_rows[...]
 
-    def arrived(ref, count, sem):
-        some = ref.at[pl.ds(0, count)]
-        pltpu.make_async_copy(some, some, sem).wait()
-
-    sent = arrived
-    if tp_count > 1:
-        arrived(wo, tp_count - 1, recv_sems.at[5])
-
-    with jax.named_scope("wait_rows"):
-        mine_too = jnp.logical_and(owner, own_to == tp)
-
-        @pl.when(mine_too)
-        def _():
-            arrived(got_v, tp_count * per - 1, recv_sems.at[6])
-
-        @pl.when(jnp.logical_not(mine_too))
-        def _():
-            arrived(got_v, tp_count * per, recv_sems.at[6])
-
-    total = jnp.zeros((per * PROPS, wo.shape[1]), f32)
-    for s in range(tp_count):
-        rows_in = got_rows[s].reshape(per * PROPS, WIDE)
-        total = total + dot_nt(rows_in, wo[s]).astype(bf16).astype(f32)
-    mixed_ref[...] = total.astype(bf16)
-
     @pl.when(my_z >= FIRST_WRITER)
     def _():
-        @pl.when(owner)
-        def _():
-            copy = pltpu.make_async_copy(own_new, new_ref.at[own_b], local_sems.at[14])
-            copy.start()
-            copy.wait()
-
-        @pl.loop(0, NZ)
-        def _(z):
-            for r in range(3):
-
-                @pl.when(owner_of(z, r) != me)
-                @jax.named_scope("wait_fresh")
-                def _():
-                    there = new_ref.at[z + NZ * r]
-                    pltpu.make_async_copy(there, there, new_sems.at[z + NZ * r]).wait()
+        with jax.named_scope("wait_column"):
+
+            @pl.when(owner)
+            def _():
+                arrived(new_ref, SEQS // NX - 1, recv_sems.at[6])
+
+            @pl.when(jnp.logical_not(owner))
+            def _():
+                arrived(new_ref, SEQS // NX, recv_sems.at[6])
+
+        def pass_on(b, z):
+            for k in range(1, NX):
+                there = {"kv": my_z * NX + lax.rem(my_x + k, NX)}
+                remote(
+                    new_ref.at[b], new_ref.at[b], send_sems.at[10], recv_sems.at[8], there
+                ).start()
+
+        in_column(pass_on)
 
     def sent_to_owners(count):
         sent(part_q, count, send_sems.at[0])
-        sent(got_s, count, send_sems.at[1])
-        sent(part_n, count, send_sems.at[2])
+        sent(part_s, count, send_sems.at[1])
         sent(out_s, count, send_sems.at[4])
         sent(out_v, count, send_sems.at[5])
+        sent(got_x, count - SEQS // NX * (NX - 1), send_sems.at[9])
+
+    sent(got_x, SEQS - SEQS // NX, send_sems.at[2])
 
     @pl.when(owner)
     def _():
@@ -525,15 +571,13 @@
         def _():
             sent(got_v, NKV, send_sems.at[7])
 
-        writers = NKV - NX * FIRST_WRITER
-
         @pl.when(my_z >= FIRST_WRITER)
         def _():
-            sent(part_n, writers - 1, send_sems.at[6])
+            sent(got_x, NZ - FIRST_WRITER - 1, send_sems.at[6])
 
         @pl.when(my_z < FIRST_WRITER)
         def _():
-            sent(part_n, writers, send_sems.at[6])
+            sent(got_x, NZ - FIRST_WRITER, send_sems.at[6])
 
     @pl.when(jnp.logical_not(owner))
     def _():
@@ -546,6 +590,38 @@
             pl.semaphore_wait(planes_in, tp_count - 1)
 
         sent(wo, tp_count - 1, send_sems.at[8])
+
+    @pl.when(my_z >= FIRST_WRITER)
+    def _():
+        sent(got_x, SEQS - SEQS // NX, send_sems.at[10])
+
+        with jax.named_scope("wait_fresh"):
+            arrived(new_ref, SEQS - SEQS // NX, recv_sems.at[8])
+
+    if tp_count > 1:
+        arrived(wo, tp_count - 1, recv_sems.at[5])
+
+    total = jnp.zeros((per * PROPS, wo.shape[1]), f32)
+    for k in range(tp_count):
+        plane = lax.rem(tp + k, tp_count)
+        with jax.named_scope("wait_rows"):
+            if k == 0:
+                mine_too = jnp.logical_and(owner, own_to == tp)
+
+                @pl.when(mine_too)
+                def _():
+                    arrived(got_v, per - 1, row_sems.at[plane])
+
+                @pl.when(jnp.logical_not(mine_too))
+                def _():
+                    arrived(got_v, per, row_sems.at[plane])
+
+            else:
+                arrived(got_v, per, row_sems.at[plane])
+        with jax.named_scope("project"):
+            rows_in = got_rows[plane].reshape(per * PROPS, WIDE)
+            total = total + dot_nt(rows_in, wo[plane])
+    mixed_ref[...] = total.astype(bf16)
 
 
 def write_kernel(
@@ -557,7 +633,7 @@
     both = ((keys, keys_out), (values, values_out))
 
     def copy_out(k, b):
-        return pltpu.make_async_copy(both[k][0].at[b], both[k][1].at[b], sems_out.at[k, b])
+        return pltpu.make_async_copy(both[k][0].at[b], both[k][1].at[b], sems_out.at[k])
 
     mixed = pltpu.make_async_copy(mixed_in, mixed_out, sem_mixed)
     mixed.start()
@@ -584,10 +660,10 @@
         for k in range(2):
             copy_out(k, b).start()
 
-    @pl.loop(0, SEQS)
-    def _(b):
+    with jax.named_scope("write_wait"):
+
         for k in range(2):
-            copy_out(k, b).wait()
+            pltpu.make_async_copy(both[k][0], both[k][1], sems_out.at[k]).wait()
 
     mixed.wait()
 
@@ -637,7 +713,9 @@
             pltpu.VMEM((SEQS, PROPS, 2 * WIDE), bf16),
             pltpu.VMEM((SEQS, 1, WIDE), f32),
             pltpu.VMEM((NKV, PROPS, WIDE), bf16),
-            pltpu.VMEM((NKV, PROPS, 2 * WIDE), bf16),
+            pltpu.VMEM((NZ * NX, PROPS, 2 * WIDE), bf16),
+            pltpu.VMEM((NZ, PROPS, 2 * WIDE), bf16),
+            pltpu.VMEM((NZ, PROPS, 2 * WIDE), bf16),
             pltpu.VMEM((NKV, 1, WIDE), f32),
             pltpu.VMEM((SEQS, PROPS, WIDE), bf16),
             pltpu.VMEM((PROPS, 2 * WIDE), bf16),
@@ -648,11 +726,11 @@
             pltpu.VMEM((PROPS, WIDE), bf16),
             pltpu.VMEM((tp_count, SEQS // tp_count, PROPS, WIDE), bf16),
             pltpu.VMEM((WIDE, WIDE), f32),
-            dma((15,)),
+            dma((14,)),
+            dma((11,)),
             dma((9,)),
-            dma((7,)),
-            dma((SEQS,)),
-            dma((SEQS,)),
+            dma((NZ,)),
+            dma((tp_count,)),
             pltpu.SemaphoreType.REGULAR,
         ],
         compiler_params=pltpu.CompilerParams(
@@ -681,7 +759,7 @@
         ),
         in_specs=[vmem, vmem, smem, smem, vmem, vmem],
         out_specs=(any_, any_, any_),
-        scratch_shapes=[dma((2, SEQS)), dma],
+        scratch_shapes=[dma((2,)), dma],
         compiler_params=pltpu.CompilerParams(vmem_limit_bytes=8 << 20),
         name="cache_write",
     )(held(mixed), held(new), prior_len, accepted, held(keys_held), held(values_held))

time: 44.9 us -> 43.3 us (0.964)
  Pallas kernels: 44.2 us -> 42.6 us
    pallas_call x1, Pallas kernels: 40.6 us -> 39.4 us  [shards(): pl.pallas_call(functools.partial(step_kernel, tp_count), out_shape=(on_ch...]
where the time goes in v3:
time: 43.3 us
  Pallas kernels  42.6 us (98%)
  between operations  0.68 us (2%)
    pallas_call x1, Pallas kernels, shards(): pl.pallas_call(functools.partial(step_kernel, tp_count), out_shape=(on_ch...  39.4 us
    pallas_call x1, Pallas kernels, shards(): pl.pallas_call(write_kernel, out_shape=(jax.ShapeDtypeStruct((out_rows, c...  3.2 us

profile of v3, /device:TPU:1, one launch (start us, length us, event | category | flops | bytes accessed | tf_op | source)
XLA Modules:
  0.0 43.3 jit_solution(14760899013889605469)
XLA Ops:
  0.6 0.0 copy-start
  0.6 0.0 copy-start.1
  0.7 39.4 %tree_step.1 = (bf16[48,64]{1,0:T(8,128)(2,1)S(1)}, bf16[24,16,256]{2,1,0:T(8,128)(2,1)S(1)}, bf16[24,512,128]{2,1,0:T(8,128)(2,1)S(1)}, bf16[24,512,128]{2,1,0:T(8,128)(2,1)S(1)}) custom-call(bf16[64,384]{1,0:T(8,128)(2,1)} %bitcast.6, f32[1,64]{1,0:T(1,128)} %bitcast.9, bf16[64,128]{1,0:T(8,128)(2,1)} %wq_hbm.1, bf16[64,128]{1,0:T(8,128)(2,1)} %wk_hbm.1, ...), custom_call_target="tpu_custom_call" | custom-call | tf_op jit(solution)/shard_map/tree_step/pallas_call | solution.py:688
  40.0 0.0 copy-done
  40.1 0.0 copy-done.1
  40.1 3.2 %cache_write.1 = (bf16[48,64]{1,0:T(8,128)(2,1)}, bf16[24,512,128]{2,1,0:T(8,128)(2,1)}, bf16[24,512,128]{2,1,0:T(8,128)(2,1)}) custom-call(bf16[48,64]{1,0:T(8,128)(2,1)S(1)} %get-tuple-element.7.mixed_in, bf16[24,16,256]{2,1,0:T(8,128)(2,1)S(1)} %get-tuple-element.8.new_ref, s32[24]{0:T(128)S(1)} %copy-done, s32[24]{0:T(128)S(1)} %copy-done.1, ...), custom_call_target="tpu_custom_call" | custom-call | tf_op jit(solution)/shard_map/cache_write/pallas_call | solution.py:753
Async XLA Ops:
  0.6 39.4 %copy-start = (s32[24]{0:T(128)S(1)}, s32[24]{0:T(128)}, u32[]{:S(2)}) copy-start(s32[24]{0:T(128)} %prior_ref.1) | copy-start | bytes 292
  0.6 39.4 %copy-start.1 = (s32[24]{0:T(128)S(1)}, s32[24]{0:T(128)}, u32[]{:S(2)}) copy-start(s32[24]{0:T(128)} %accepted_ref.1) | copy-start | bytes 292

commit v4 on v3

--- a/solution.py
+++ b/solution.py
@@ -91,6 +91,7 @@
     new_ref,
     keys,
     values,
+    filled_ref,
     bias_ref,
     prior_ref,
     accepted_ref,
@@ -331,6 +332,9 @@
             load.wait()
     positions = offset + iota((1, length), 1)
 
+    for b in range(SEQS):
+        filled_ref[b] = prior_ref[b] + accepted_ref[b]
+
     with jax.named_scope("prepare"):
 
         @pl.loop(0, SEQS)
@@ -391,9 +395,9 @@
     with jax.named_scope("wait_cache"):
         loads[12].wait()
 
-    @pl.loop(0, NZ // 2)
+    @pl.loop(0, NZ // 4)
     def _(i):
-        pair = [lax.rem(my_z + near_first(2 * i + k), NZ) for k in range(2)]
+        pair = [lax.rem(my_z + far_first(4 * i + k), NZ) for k in range(4)]
         for z in pair:
             with jax.named_scope("wait_query"):
                 mine_too = jnp.logical_and(owner, z == my_z)
@@ -625,7 +629,7 @@
 
 
 def write_kernel(
-    mixed_in, new_ref, prior_ref, accepted_ref, keys, values,
+    mixed_in, new_ref, filled_ref, keys, values,
     mixed_out, keys_out, values_out, sems_out, sem_mixed,
 ):
     me = lax.axis_index("kv")
@@ -640,7 +644,7 @@
 
     @pl.loop(0, SEQS)
     def _(b):
-        start = prior_ref[b] + accepted_ref[b] - me * length
+        start = filled_ref[b] - me * length
 
         @pl.when((start > -PROPS) & (start < length))
         def _():
@@ -670,6 +674,10 @@
 
 def on_chip(shape, dtype):
     return pltpu.VMEM(shape, dtype)
+
+
+def scalars(shape, dtype):
+    return pltpu.SMEM(shape, dtype)
 
 
 def shards(
@@ -685,16 +693,17 @@
     vmem = pl.BlockSpec(memory_space=pltpu.VMEM)
     out_rows = rows // tp_count
     dma = pltpu.SemaphoreType.DMA
-    mixed, new, keys_held, values_held = pl.pallas_call(
+    mixed, new, keys_held, values_held, filled = pl.pallas_call(
         functools.partial(step_kernel, tp_count),
         out_shape=(
             on_chip((out_rows, columns), bf16),
             on_chip((SEQS, PROPS, 2 * WIDE), bf16),
             on_chip(keys_cache.shape, bf16),
             on_chip(values_cache.shape, bf16),
+            scalars(prior_len.shape, jnp.int32),
         ),
         in_specs=[pl.BlockSpec(memory_space=pltpu.HBM)] * 14,
-        out_specs=(vmem, vmem, vmem, vmem),
+        out_specs=(vmem, vmem, vmem, vmem, smem),
         scratch_shapes=[
             pltpu.SMEM(gate_bias.shape, f32),
             pltpu.SMEM(prior_len.shape, jnp.int32),
@@ -757,12 +766,18 @@
             jax.ShapeDtypeStruct(keys_cache.shape, bf16),
             jax.ShapeDtypeStruct(values_cache.shape, bf16),
         ),
-        in_specs=[vmem, vmem, smem, smem, vmem, vmem],
+        in_specs=[vmem, vmem, smem, vmem, vmem],
         out_specs=(any_, any_, any_),
         scratch_shapes=[dma((2,)), dma],
         compiler_params=pltpu.CompilerParams(vmem_limit_bytes=8 << 20),
         name="cache_write",
-    )(held(mixed), held(new), prior_len, accepted, held(keys_held), held(values_held))
+    )(
+        held(mixed),
+        held(new),
+        pltpu.with_memory_space_constraint(filled, pltpu.SMEM),
+        held(keys_held),
+        held(values_held),
+    )
 
 
 def solution(mesh):

time: 43.3 us -> 41.9 us (0.968)
  Pallas kernels: 42.6 us -> 41.1 us
    pallas_call x1, Pallas kernels: 39.4 us -> 38.4 us  [shards(): pl.pallas_call(functools.partial(step_kernel, tp_count), out_shape=(on_ch...]
    pallas_call x1, Pallas kernels: 3.2 us -> 2.65 us  [shards(): pl.pallas_call(write_kernel, out_shape=(jax.ShapeDtypeStruct((out_rows, c...]
where the time goes in v4:
time: 41.9 us; the launch traced here: 41.7 us
  Pallas kernels  41.1 us (98%)
  between operations  0.64 us (2%)
    pallas_call x1, Pallas kernels, shards(): pl.pallas_call(functools.partial(step_kernel, tp_count), out_shape=(on_ch...  38.4 us
    pallas_call x1, Pallas kernels, shards(): pl.pallas_call(write_kernel, out_shape=(jax.ShapeDtypeStruct((out_rows, c...  2.65 us

profile of v4, /device:TPU:1, one launch (start us, length us, event | category | flops | bytes accessed | tf_op | source)
XLA Modules:
  0.0 41.7 jit_solution(12374384274199353619)
XLA Ops:
  0.6 38.4 %tree_step.1 = (bf16[48,64]{1,0:T(8,128)(2,1)S(1)}, bf16[24,16,256]{2,1,0:T(8,128)(2,1)S(1)}, bf16[24,512,128]{2,1,0:T(8,128)(2,1)S(1)}, bf16[24,512,128]{2,1,0:T(8,128)(2,1)S(1)}, s32[24]{0:T(128)S(4)}) custom-call(bf16[64,384]{1,0:T(8,128)(2,1)} %bitcast.6, f32[1,64]{1,0:T(1,128)} %bitcast.9, bf16[64,128]{1,0:T(8,128)(2,1)} %wq_hbm.1, ...), custom_call_target="tpu_custom_call" | custom-call | tf_op jit(solution)/shard_map/tree_step/pallas_call | solution.py:696
  39.1 2.7 %cache_write.1 = (bf16[48,64]{1,0:T(8,128)(2,1)}, bf16[24,512,128]{2,1,0:T(8,128)(2,1)}, bf16[24,512,128]{2,1,0:T(8,128)(2,1)}) custom-call(bf16[48,64]{1,0:T(8,128)(2,1)S(1)} %get-tuple-element.8.mixed_in, bf16[24,16,256]{2,1,0:T(8,128)(2,1)S(1)} %get-tuple-element.9.new_ref, s32[24]{0:T(128)S(4)} %get-tuple-element.10.filled_ref, ...), custom_call_target="tpu_custom_call" | custom-call | tf_op jit(solution)/shard_map/cache_write/pallas_call | solution.py:762

commit v5 on v4

--- a/solution.py
+++ b/solution.py
@@ -37,13 +37,8 @@
     return 4 + (1 - 2 * lax.rem(i, 2)) * lax.div(i + 1, 2)
 
 
-def near_first(i):
-    odd = lax.rem(i, 2)
-    return odd * lax.div(i + 1, 2) + (1 - odd) * lax.rem(NZ - lax.div(i, 2), NZ)
-
-
-def owner_of(z, r):
-    return z * NX + lax.rem(z + 1 + r, NX)
+def sequence_at(z, x):
+    return lax.rem(z, 4) + 4 * x + 16 * lax.div(z, 4)
 
 
 def split_heads(rows):
@@ -132,26 +127,35 @@
     me = lax.axis_index("kv")
     tp = lax.axis_index("tp")
     my_z, my_x = lax.div(me, NX), lax.rem(me, NX)
-    my_r = lax.rem(my_x - my_z - 1 + 2 * NX * NZ, NX)
-    owner = my_r < 3
-    own_b = lax.min(my_z + NZ * my_r, SEQS - 1)
+    owner = sequence_at(my_z, my_x) < SEQS
+    own_b = lax.min(sequence_at(my_z, my_x), SEQS - 1)
+    broad = my_x < 2
     per = SEQS // tp_count
     own_to = lax.div(own_b, per)
+    half = max(1, tp_count // 2)
     length = keys.shape[1]
     offset = me * length
     heads = 2
 
     barrier = pltpu.get_barrier_semaphore()
 
-    @pl.loop(0, NZ)
-    def _(i):
-        z = lax.rem(my_z + far_first(i), NZ)
-        for k in range(NX):
-            peer = z * NX + lax.rem(my_x + (2, 1, 3, 0)[k], NX)
-
-            @pl.when(peer != me)
-            def _():
-                pl.semaphore_signal(barrier, inc=1, device_id={"kv": peer})
+    @pl.when(owner)
+    def _():
+        @pl.loop(0, NZ)
+        def _(i):
+            z = lax.rem(my_z + far_first(i), NZ)
+            for k in range(NX):
+                peer = z * NX + lax.rem(my_x + (2, 1, 3, 0)[k], NX)
+
+                @pl.when(peer != me)
+                def _():
+                    pl.semaphore_signal(barrier, inc=1, device_id={"kv": peer})
+
+    @pl.when(jnp.logical_not(owner))
+    def _():
+        for k in range(1, NX):
+            peer = my_z * NX + lax.rem(my_x + k, NX)
+            pl.semaphore_signal(barrier, inc=1, device_id={"kv": peer})
 
     @pl.loop(0, tp_count - 1)
     def _(i):
@@ -228,7 +232,8 @@
     part_n[:, :, WIDE:] = dot_nn(scaled, wv[...]).astype(bf16).reshape(SEQS, PROPS, WIDE)
 
     with jax.named_scope("barrier"):
-        pl.semaphore_wait(barrier, NKV - 1 + tp_count - 1)
+        beside = jnp.where(my_z >= 4, 2, 0)
+        pl.semaphore_wait(barrier, SEQS - 1 + beside + tp_count - 1)
 
     def remote(src, dst, send, recv, where):
         return pltpu.make_async_remote_copy(
@@ -239,30 +244,28 @@
         @pl.loop(0, NZ)
         def _(i):
             z = lax.rem(my_z + far_first(i), NZ)
-            for r in range(3):
-                peer = owner_of(z, r)
-
-                @pl.when(peer != me)
+            for x_at in range(NX):
+                peer = z * NX + x_at
+                b = sequence_at(z, x_at)
+
+                @pl.when(jnp.logical_and(b < SEQS, peer != me))
                 def _():
-                    body(z + NZ * r, peer)
-
-    def to_everyone(low, body):
+                    body(lax.min(b, SEQS - 1), peer)
+
+    def to_everyone(body):
         @pl.loop(0, NZ)
         def _(i):
             z = lax.rem(my_z + far_first(i), NZ)
-
-            @pl.when(z >= low)
-            def _():
-                for k in range(NX):
-                    body(z * NX + lax.rem(my_x + (2, 1, 3, 0)[k], NX))
-
-    def to_all(low, body):
-        def other(peer):
+            for k in range(NX):
+                body(z * NX + lax.rem(my_x + (2, 1, 3, 0)[k], NX), i)
+
+    def to_all(body):
+        def other(peer, i):
             @pl.when(peer != me)
             def _():
-                body(peer)
-
-        to_everyone(low, other)
+                body(peer, i)
+
+        to_everyone(other)
 
     def send_queries(b, peer):
         remote(part_q.at[b], got_q.at[me], send_sems.at[0], recv_sems.at[0], {"kv": peer}).start()
@@ -271,18 +274,22 @@
     def along_x(body):
         @pl.loop(0, NZ)
         def _(z):
-            for r in range(3):
-                body(z + NZ * r, z, lax.rem(z + 1 + r, NX))
+            for x_at in range(NX):
+                b = sequence_at(z, x_at)
+
+                @pl.when(b < SEQS)
+                def _():
+                    body(lax.min(b, SEQS - 1), z, x_at)
 
     def in_column(body):
         @pl.loop(0, NZ)
         def _(i):
             z = lax.rem(my_z + far_first(i), NZ)
-            r = lax.rem(my_x - z - 1 + 2 * NX * NZ, NX)
-
-            @pl.when(r < 3)
+            b = sequence_at(z, my_x)
+
+            @pl.when(b < SEQS)
             def _():
-                body(lax.min(z + NZ * r, SEQS - 1), z)
+                body(lax.min(b, SEQS - 1), z)
 
     def send_new(b, z, x_at):
         slot = NX * z + my_x
@@ -322,7 +329,6 @@
     @pl.loop(0, tp_count - 1)
     def _(i):
         there = {"tp": lax.rem(tp + i + 1, tp_count)}
-        pl.semaphore_signal(planes_in, inc=1, device_id=there)
         remote(wo.at[tp], wo.at[tp], send_sems.at[8], recv_sems.at[5], there).start()
 
     along_x(send_new)
@@ -356,6 +362,15 @@
 
     sent = arrived
 
+    def of_column(ref, count, other, sem):
+        @pl.when(broad)
+        def _():
+            arrived(ref, count, sem)
+
+        @pl.when(jnp.logical_not(broad))
+        def _():
+            arrived(ref, other, sem)
+
     def all_arrived(ref, sem):
         arrived(ref, NKV - 1, sem)
 
@@ -375,42 +390,39 @@
         rounded = (inverse * total).astype(bf16).astype(f32)
         queries[own_b] = (rounded * HEAD**-0.5).astype(bf16)
 
-        def send(peer):
+        def send(peer, i):
+            step = lax.rem(far_first(i), 4)
+            part = jnp.where(step == 0, 0, jnp.where(step == 2, 2, 1))
             remote(
                 queries.at[own_b],
                 queries.at[own_b],
                 send_sems.at[3],
-                query_sems.at[my_z],
+                query_sems.at[part],
                 {"kv": peer},
             ).start()
 
         with jax.named_scope("send_queries"):
-            to_all(0, send)
+            to_all(send)
+
+        @pl.loop(0, tp_count - 1)
+        def _(i):
+            there = {"tp": lax.rem(tp + i + 1, tp_count)}
+            pl.semaphore_signal(planes_in, inc=1, device_id=there)
 
     with jax.named_scope("pass_new"):
-        arrived(got_x, SEQS - SEQS // NX, recv_sems.at[2])
+        of_column(got_x, 24, 12, recv_sems.at[2])
         in_column(pass_new)
         in_column(send_sums)
 
     with jax.named_scope("wait_cache"):
         loads[12].wait()
 
-    @pl.loop(0, NZ // 4)
-    def _(i):
-        pair = [lax.rem(my_z + far_first(4 * i + k), NZ) for k in range(4)]
-        for z in pair:
-            with jax.named_scope("wait_query"):
-                mine_too = jnp.logical_and(owner, z == my_z)
-
-                @pl.when(mine_too)
-                def _():
-                    arrived(queries, 2, query_sems.at[z])
-
-                @pl.when(jnp.logical_not(mine_too))
-                def _():
-                    arrived(queries, 3, query_sems.at[z])
-
-        group = [(z + NZ * r, owner_of(z, r)) for z in pair for r in range(3)]
+    def attend(steps):
+        group = []
+        for step in steps:
+            z = lax.rem(my_z + step, 4)
+            group += [(z + 4 * x_at, z * NX + x_at) for x_at in range(4)]
+            group += [(z + 4 * x_at + 16, (z + 4) * NX + x_at) for x_at in range(2)]
         scores = []
         for b, _ in group:
             bias = cum[b]
@@ -438,6 +450,24 @@
                 remote(
                     out_v.at[b], got_v.at[me], send_sems.at[5], recv_sems.at[4], there
                 ).start()
+
+    with jax.named_scope("wait_query"):
+
+        @pl.when(owner)
+        def _():
+            arrived(queries, 5, query_sems.at[0])
+
+        @pl.when(jnp.logical_not(owner))
+        def _():
+            arrived(queries, 6, query_sems.at[0])
+
+    attend((0,))
+    with jax.named_scope("wait_query"):
+        arrived(queries, 12, query_sems.at[1])
+    attend((1, 3))
+    with jax.named_scope("wait_query"):
+        arrived(queries, 6, query_sems.at[2])
+    attend((2,))
 
     @pl.when(owner)
     def _():
@@ -499,34 +529,35 @@
         factors = jnp.exp(jnp.where(held, stats - top, 0.0))
         sums_in = jnp.concatenate([stats[:, :, 32:], stats[:, :, :32]], axis=2)
         grand = jnp.sum(factors * sums_in, axis=0, keepdims=True)
-        shares = factors / jnp.where(held, grand, 1.0)
+        inverse_grand = 1.0 / jnp.where(held, grand, 1.0)[0]
         with jax.named_scope("wait_blocks"):
             all_arrived(got_v, recv_sems.at[4])
         first = iota((PROPS, WIDE), 1) < HEAD
         result = jnp.zeros((PROPS, WIDE), f32)
         for s in range(NKV + 1):
-            share = shares[s]
+            share = factors[s]
             pair = jnp.where(first, as_column(share, 0), as_column(share, PROPS))
             result = result + pair * got_v[s].astype(f32)
-        own_rows[...] = result.astype(bf16)
+        whole = jnp.where(first, as_column(inverse_grand, 0), as_column(inverse_grand, PROPS))
+        own_rows[...] = (result * whole).astype(bf16)
         slot = lax.rem(own_b, per)
 
         if tp_count > 1:
             pl.semaphore_wait(planes_in, tp_count - 1)
 
-        def send_rows(peer):
+        def send_rows(peer, step):
             @pl.when(jnp.logical_or(peer != me, own_to != tp))
             def _():
                 remote(
                     own_rows,
                     got_rows.at[tp, slot],
                     send_sems.at[7],
-                    row_sems.at[tp],
+                    row_sems.at[lax.div(lax.rem(tp - own_to + tp_count, tp_count), half)],
                     {"kv": peer, "tp": own_to},
                 ).start()
 
         with jax.named_scope("send_rows"):
-            to_everyone(0, send_rows)
+            to_everyone(send_rows)
 
         @pl.when(own_to == tp)
         def _():
@@ -536,13 +567,7 @@
     def _():
         with jax.named_scope("wait_column"):
 
-            @pl.when(owner)
-            def _():
-                arrived(new_ref, SEQS // NX - 1, recv_sems.at[6])
-
-            @pl.when(jnp.logical_not(owner))
-            def _():
-                arrived(new_ref, SEQS // NX, recv_sems.at[6])
+            of_column(new_ref, 7, 4, recv_sems.at[6])
 
         def pass_on(b, z):
             for k in range(1, NX):
@@ -558,9 +583,9 @@
         sent(part_s, count, send_sems.at[1])
         sent(out_s, count, send_sems.at[4])
         sent(out_v, count, send_sems.at[5])
-        sent(got_x, count - SEQS // NX * (NX - 1), send_sems.at[9])
-
-    sent(got_x, SEQS - SEQS // NX, send_sems.at[2])
+        of_column(got_x, 8 - SEQS + count, 4 - SEQS + count, send_sems.at[9])
+
+    of_column(got_x, 16, 20, send_sems.at[2])
 
     @pl.when(owner)
     def _():
@@ -588,40 +613,36 @@
         sent_to_owners(SEQS)
 
     if tp_count > 1:
-
-        @pl.when(jnp.logical_not(owner))
-        def _():
-            pl.semaphore_wait(planes_in, tp_count - 1)
-
         sent(wo, tp_count - 1, send_sems.at[8])
 
     @pl.when(my_z >= FIRST_WRITER)
     def _():
-        sent(got_x, SEQS - SEQS // NX, send_sems.at[10])
+        of_column(got_x, 24, 12, send_sems.at[10])
 
         with jax.named_scope("wait_fresh"):
-            arrived(new_ref, SEQS - SEQS // NX, recv_sems.at[8])
+            of_column(new_ref, 16, 20, recv_sems.at[8])
 
     if tp_count > 1:
         arrived(wo, tp_count - 1, recv_sems.at[5])
 
     total = jnp.zeros((per * PROPS, wo.shape[1]), f32)
+    mine_too = jnp.logical_and(owner, own_to == tp)
     for k in range(tp_count):
         plane = lax.rem(tp + k, tp_count)
-        with jax.named_scope("wait_rows"):
-            if k == 0:
-                mine_too = jnp.logical_and(owner, own_to == tp)
+        if k == 0:
+            with jax.named_scope("wait_rows"):
 
                 @pl.when(mine_too)
                 def _():
-                    arrived(got_v, per - 1, row_sems.at[plane])
+                    arrived(got_v, half * per - 1, row_sems.at[0])
 
                 @pl.when(jnp.logical_not(mine_too))
                 def _():
-                    arrived(got_v, per, row_sems.at[plane])
-
-            else:
-                arrived(got_v, per, row_sems.at[plane])
+                    arrived(got_v, half * per, row_sems.at[0])
+
+        elif k == half:
+            with jax.named_scope("wait_rows"):
+                arrived(got_v, (tp_count - half) * per, row_sems.at[1])
         with jax.named_scope("project"):
             rows_in = got_rows[plane].reshape(per * PROPS, WIDE)
             total = total + dot_nt(rows_in, wo[plane])
@@ -738,8 +759,8 @@
             dma((14,)),
             dma((11,)),
             dma((9,)),
-            dma((NZ,)),
-            dma((tp_count,)),
+            dma((3,)),
+            dma((2,)),
             pltpu.SemaphoreType.REGULAR,
         ],
         compiler_params=pltpu.CompilerParams(

time: 41.9 us -> 39.6 us (0.945)
  Pallas kernels: 41.1 us -> 38.8 us
    pallas_call x1, Pallas kernels: 38.4 us -> 36.2 us  [shards(): pl.pallas_call(functools.partial(step_kernel, tp_count), out_shape=(on_ch...]
where the time goes in v5:
time: 39.6 us; the launch traced here: 39.5 us
  Pallas kernels  38.8 us (98%)
  between operations  0.64 us (2%)
    pallas_call x1, Pallas kernels, shards(): pl.pallas_call(functools.partial(step_kernel, tp_count), out_shape=(on_ch...  36.2 us
    pallas_call x1, Pallas kernels, shards(): pl.pallas_call(write_kernel, out_shape=(jax.ShapeDtypeStruct((out_rows, c...  2.65 us

profile of v5, /device:TPU:1, one launch (start us, length us, event | category | flops | bytes accessed | tf_op | source)
XLA Modules:
  0.0 39.5 jit_solution(15876581312981901136)
XLA Ops:
  0.6 36.2 %tree_step.1 = (bf16[48,64]{1,0:T(8,128)(2,1)S(1)}, bf16[24,16,256]{2,1,0:T(8,128)(2,1)S(1)}, bf16[24,512,128]{2,1,0:T(8,128)(2,1)S(1)}, bf16[24,512,128]{2,1,0:T(8,128)(2,1)S(1)}, s32[24]{0:T(128)S(4)}) custom-call(bf16[64,384]{1,0:T(8,128)(2,1)} %bitcast.6, f32[1,64]{1,0:T(1,128)} %bitcast.9, bf16[64,128]{1,0:T(8,128)(2,1)} %wq_hbm.1, ...), custom_call_target="tpu_custom_call" | custom-call | tf_op jit(solution)/shard_map/tree_step/pallas_call | solution.py:717
  36.8 2.7 %cache_write.1 = (bf16[48,64]{1,0:T(8,128)(2,1)}, bf16[24,512,128]{2,1,0:T(8,128)(2,1)}, bf16[24,512,128]{2,1,0:T(8,128)(2,1)}) custom-call(bf16[48,64]{1,0:T(8,128)(2,1)S(1)} %get-tuple-element.8.mixed_in, bf16[24,16,256]{2,1,0:T(8,128)(2,1)S(1)} %get-tuple-element.9.new_ref, s32[24]{0:T(128)S(4)} %get-tuple-element.10.filled_ref, ...), custom_call_target="tpu_custom_call" | custom-call | tf_op jit(solution)/shard_map/cache_write/pallas_call | solution.py:783

commit v6 on v5

--- a/solution.py
+++ b/solution.py
@@ -392,7 +392,7 @@
 
         def send(peer, i):
             step = lax.rem(far_first(i), 4)
-            part = jnp.where(step == 0, 0, jnp.where(step == 2, 2, 1))
+            part = jnp.where(step == 0, 0, 1)
             remote(
                 queries.at[own_b],
                 queries.at[own_b],
@@ -463,11 +463,8 @@
 
     attend((0,))
     with jax.named_scope("wait_query"):
-        arrived(queries, 12, query_sems.at[1])
-    attend((1, 3))
-    with jax.named_scope("wait_query"):
-        arrived(queries, 6, query_sems.at[2])
-    attend((2,))
+        arrived(queries, 18, query_sems.at[1])
+    attend((1, 3, 2))
 
     @pl.when(owner)
     def _():
@@ -759,7 +756,7 @@
             dma((14,)),
             dma((11,)),
             dma((9,)),
-            dma((3,)),
+            dma((2,)),
             dma((2,)),
             pltpu.SemaphoreType.REGULAR,
         ],

time: 39.6 us -> 39.9 us (level)
  no operation moved by 1% of the time
where the time goes in v6:
time: 39.9 us; the launch traced here: 39.8 us
  Pallas kernels  39.1 us (98%)
  between operations  0.64 us (2%)
    pallas_call x1, Pallas kernels, shards(): pl.pallas_call(functools.partial(step_kernel, tp_count), out_shape=(on_ch...  36.5 us
    pallas_call x1, Pallas kernels, shards(): pl.pallas_call(write_kernel, out_shape=(jax.ShapeDtypeStruct((out_rows, c...  2.65 us

profile of v6, /device:TPU:1, one launch (start us, length us, event | category | flops | bytes accessed | tf_op | source)
XLA Modules:
  0.0 39.8 jit_solution(7973513436921865803)
XLA Ops:
  0.6 36.5 %tree_step.1 = (bf16[48,64]{1,0:T(8,128)(2,1)S(1)}, bf16[24,16,256]{2,1,0:T(8,128)(2,1)S(1)}, bf16[24,512,128]{2,1,0:T(8,128)(2,1)S(1)}, bf16[24,512,128]{2,1,0:T(8,128)(2,1)S(1)}, s32[24]{0:T(128)S(4)}) custom-call(bf16[64,384]{1,0:T(8,128)(2,1)} %bitcast.6, f32[1,64]{1,0:T(1,128)} %bitcast.9, bf16[64,128]{1,0:T(8,128)(2,1)} %wq_hbm.1, ...), custom_call_target="tpu_custom_call" | custom-call | tf_op jit(solution)/shard_map/tree_step/pallas_call | solution.py:714
  37.1 2.7 %cache_write.1 = (bf16[48,64]{1,0:T(8,128)(2,1)}, bf16[24,512,128]{2,1,0:T(8,128)(2,1)}, bf16[24,512,128]{2,1,0:T(8,128)(2,1)}) custom-call(bf16[48,64]{1,0:T(8,128)(2,1)S(1)} %get-tuple-element.8.mixed_in, bf16[24,16,256]{2,1,0:T(8,128)(2,1)S(1)} %get-tuple-element.9.new_ref, s32[24]{0:T(128)S(4)} %get-tuple-element.10.filled_ref, ...), custom_call_target="tpu_custom_call" | custom-call | tf_op jit(solution)/shard_map/cache_write/pallas_call | solution.py:780
